TPU v7x, 128 devices: a whole 4x4x4 slice. The times are simulated.
128 devices in a mesh: ep: 32 (over z, y, core), tp: 4 (over x).
Axes of the slice: x: 4, y: 4, z: 4, core: 2. Of those that a mesh axis runs over, the one named last changes fastest.
Arguments:
- mixer_input: bfloat16 [16384, 2048], P('ep'), may hold values from -6 to 6
- log_forget_total: float32 [16, 16384], P('tp'), may hold values from -2732 to 0, as said below
- mixer_gain: float32 [2048], replicated, may hold values from 0.1 to 1.9
- w_query: bfloat16 [2048, 1024], P(None, 'tp'), may hold values from -1 to 1
- w_key: bfloat16 [2048, 256], P(None, 'tp'), may hold values from -8 to 8
- w_value: bfloat16 [2048, 256], P(None, 'tp'), may hold values from -0.125 to 0.125
- w_output: bfloat16 [1024, 2048], replicated, may hold values from -0.1875 to 0.1875
- mixer_post_gain: float32 [2048], replicated, may hold values from 0.1 to 1.9
- expert_input: bfloat16 [8192, 2048], P('ep'), may hold values from -6 to 6
- expert_ids: int32 [8192, 2], P('ep'), may hold values from 0 to 31, all different within a row; in each aligned block of 64 rows (0 to 63, 64 to 127, ...) at most 8 rows name the same one
- route_weight: float32 [8192, 2], P('ep'), may hold values from 0.1 to 1
- expert_gain: float32 [2048], replicated, may hold values from 0.1 to 1.9
- w_gate: bfloat16 [32, 2048, 3584], P('ep', None, 'tp'), may hold values from -0.125 to 0.125
- w_up: bfloat16 [32, 2048, 3584], P('ep', None, 'tp'), may hold values from -0.125 to 0.125
- w_down: bfloat16 [32, 3584, 2048], P('ep', 'tp'), may hold values from -0.09375 to 0.09375
- expert_post_gain: float32 [2048], replicated, may hold values from 0.1 to 1.9
Outputs:
- mixer_out: bfloat16 [16384, 2048], P(('ep', 'tp'))
- expert_out: bfloat16 [8192, 2048], P(('ep', 'tp'))
Inputs may be any that keep to these rules, and one draw needn't show every extreme that they name: `expert_ids`: in each aligned block of 64 tokens no expert is named by more than 8 of them. `log_forget_total`: each head's values never rise along the positions.
All inputs are finite; a program needn't handle non-finite values.
Results may differ from a plain program's by a relative error of at most 0.012.
The roundings to bfloat16 on the way count: a program that leaves them out, or rounds other values in their place, can miss the bound.
Values may be sent and summed in bfloat16 or wider, within the bound.
A program may use at most 128 MiB of HBM per device.

v0:
```python
import math

import jax
import jax.numpy as jnp
from jax import lax
from jax.sharding import PartitionSpec as P

HD = 64
TOP_K = 2


NEG_FILL = -1e30
NORM_EPS = 1e-06


def side_by_side(arrays, axis, dim, along):
    both = jnp.concatenate(arrays, axis=along)
    out, at, gathered = (lax.all_gather(both, axis, axis=dim, tiled=True), 0, [])
    for a in arrays:
        gathered.append(lax.slice_in_dim(out, at, at + a.shape[along], axis=along))
        at += a.shape[along]
    return tuple(gathered)


def norm_rows(values_in, gain_vec):
    widened = values_in.astype(jnp.float32)
    return (
        widened
        * lax.rsqrt(jnp.mean(widened * widened, axis=-1, keepdims=True) + NORM_EPS)
        * gain_vec
    )


def unchanged(present_state):
    return present_state


def mixer_half(
    mixer_input, log_forget_total, mixer_gain, w_query, w_key, w_value, w_output, mixer_post_gain
):
    row_count = mixer_input.shape[0]
    offset = lax.axis_index("ep") * row_count
    head_local = w_query.shape[1] // HD
    kv_local = w_key.shape[1] // HD
    group_size = head_local // kv_local
    normed = norm_rows(mixer_input, mixer_gain).astype(jnp.bfloat16)
    queries = (
        jnp.dot(normed, w_query, preferred_element_type=jnp.float32)
        .astype(jnp.bfloat16)
        .reshape(row_count, kv_local, group_size, HD)
    )
    key_rows = (
        jnp.dot(normed, w_key, preferred_element_type=jnp.float32)
        .astype(jnp.bfloat16)
        .reshape(row_count, kv_local, HD)
    )
    value_rows = (
        jnp.dot(normed, w_value, preferred_element_type=jnp.float32)
        .astype(jnp.bfloat16)
        .reshape(row_count, kv_local, HD)
    )
    gate_totals = log_forget_total.reshape(kv_local, group_size, -1)
    query_gate = lax.dynamic_slice_in_dim(gate_totals, offset, row_count, 2)
    query_pos = offset + jnp.arange(row_count, dtype=jnp.int32)
    last_row = offset + row_count - 1
    score_scale = HD ** (-0.5)
    start_state = (
        jnp.full((kv_local, group_size, row_count), NEG_FILL, jnp.float32),
        jnp.zeros((kv_local, group_size, row_count), jnp.float32),
        jnp.zeros((kv_local, group_size, row_count, HD), jnp.float32),
    )
    running = start_state
    key_piece, value_piece = side_by_side((key_rows, value_rows), "ep", 0, 1)
    piece_rows = key_piece.shape[0]
    block_rows = math.gcd(piece_rows, 512)
    block_total = piece_rows // block_rows
    key_blocks = key_piece.reshape(block_total, block_rows, kv_local, HD)
    value_blocks = value_piece.reshape(block_total, block_rows, kv_local, HD)

    def one_block(present_state, operands):
        key_block, value_block, block_index = operands
        block_first = block_index * block_rows

        def update(prior_value):
            row_max, denominator, numerator = prior_value
            key_gate = lax.dynamic_slice_in_dim(gate_totals, block_first, block_rows, 2)
            scores = (
                jnp.einsum("qgjd,kgd->gjqk", queries, key_block, preferred_element_type=jnp.float32)
                * score_scale
            )
            scores = scores + query_gate[:, :, :, None] - key_gate[:, :, None, :]
            visible = (block_first + jnp.arange(block_rows, dtype=jnp.int32))[None, :] <= query_pos[
                :, None
            ]
            scores = jnp.where(visible, scores, NEG_FILL)
            new_max = jnp.maximum(row_max, jnp.max(scores, axis=-1))
            shifted = jnp.where(visible, jnp.exp(scores - new_max[..., None]), 0.0)
            factor = jnp.exp(row_max - new_max)
            denominator = denominator * factor + jnp.sum(shifted, axis=-1)
            numerator = numerator * factor[..., None] + jnp.einsum(
                "gjqk,kgd->gjqd",
                shifted.astype(jnp.bfloat16),
                value_block,
                preferred_element_type=jnp.float32,
            )
            return (new_max, denominator, numerator)

        return (lax.cond(block_first <= last_row, update, unchanged, present_state), None)

    running, _ = lax.scan(
        one_block, running, (key_blocks, value_blocks, jnp.arange(block_total, dtype=jnp.int32))
    )
    row_max, denominator, numerator = running
    mixed_heads = (
        jnp.transpose(numerator / denominator[..., None], (2, 0, 1, 3))
        .reshape(row_count, head_local * HD)
        .astype(jnp.bfloat16)
    )
    by_rows = lax.all_to_all(mixed_heads, "tp", split_axis=0, concat_axis=1, tiled=True)
    projected = jnp.dot(by_rows, w_output, preferred_element_type=jnp.float32)
    return norm_rows(projected, mixer_post_gain).astype(jnp.bfloat16)


def expert_half(
    expert_input, expert_ids, route_weight, expert_gain, w_gate, w_up, w_down, expert_post_gain
):
    row_count = expert_input.shape[0]
    quarters = lax.axis_size("tp")
    experts = lax.axis_size("ep")
    quarter_rows = row_count // quarters
    slot_count = 2 * TOP_K * quarter_rows // experts
    own_quarter = lax.axis_index("tp")
    normed = norm_rows(expert_input, expert_gain).astype(jnp.bfloat16)
    padded_rows = jnp.concatenate([normed, jnp.zeros((1, normed.shape[1]), jnp.bfloat16)], axis=0)
    routed = expert_ids.reshape(quarters, quarter_rows * TOP_K)
    matches = (routed[:, :, None] == jnp.arange(experts, dtype=jnp.int32)[None, None, :]).astype(
        jnp.int32
    )
    slot_ranks = jnp.sum(jnp.cumsum(matches, axis=1) * matches, axis=2) - 1
    owners = (jnp.arange(row_count * TOP_K, dtype=jnp.int32) // TOP_K).reshape(
        quarters, quarter_rows * TOP_K
    )
    quarter_index = jnp.broadcast_to(jnp.arange(quarters, dtype=jnp.int32)[:, None], routed.shape)
    slot_table = (
        jnp.full((quarters, slot_count, experts), row_count, jnp.int32)
        .at[quarter_index, slot_ranks, routed]
        .set(owners)
    )
    gate_local = w_gate[0]
    up_local = w_up[0]
    down_local = w_down[0]
    unit_count = gate_local.shape[1]
    outgoing = padded_rows[slot_table]
    arrived = lax.all_to_all(outgoing, "ep", split_axis=2, concat_axis=2, tiled=True)
    flat_rows = arrived.reshape(-1, arrived.shape[-1])
    gate_part = jnp.dot(flat_rows, gate_local, preferred_element_type=jnp.float32)
    up_part = jnp.dot(flat_rows, up_local, preferred_element_type=jnp.float32)
    hidden = (
        (jax.nn.silu(gate_part) * up_part)
        .astype(jnp.bfloat16)
        .reshape(arrived.shape[:-1] + (unit_count,))
    )
    product = jnp.dot(
        hidden.reshape(-1, unit_count), down_local, preferred_element_type=jnp.float32
    )
    summed = lax.psum_scatter(
        product.reshape(lax.axis_size("tp") * 1, slot_count, experts, product.shape[-1]).astype(
            jnp.bfloat16
        ),
        "tp",
        scatter_dimension=0,
        tiled=True,
    ).astype(jnp.float32)
    results = summed[0].astype(jnp.bfloat16)
    returned = lax.all_to_all(results, "ep", split_axis=1, concat_axis=1, tiled=True)
    flat_results = returned.reshape(slot_count * experts, returned.shape[-1])
    own_routes = lax.dynamic_index_in_dim(routed, own_quarter, 0, keepdims=False)
    own_ranks = lax.dynamic_index_in_dim(slot_ranks, own_quarter, 0, keepdims=False)
    picked = flat_results[own_ranks * experts + own_routes].reshape(quarter_rows, TOP_K, -1)
    own_weights = lax.dynamic_slice_in_dim(
        route_weight, own_quarter * quarter_rows, quarter_rows, 0
    )
    combined = jnp.sum(own_weights[:, :, None] * picked.astype(jnp.float32), axis=1)
    return norm_rows(combined, expert_post_gain).astype(jnp.bfloat16)


def per_device(
    mixer_input,
    log_forget_total,
    mixer_gain,
    w_query,
    w_key,
    w_value,
    w_output,
    mixer_post_gain,
    expert_input,
    expert_ids,
    route_weight,
    expert_gain,
    w_gate,
    w_up,
    w_down,
    expert_post_gain,
):
    mixer_out = mixer_half(
        mixer_input,
        log_forget_total,
        mixer_gain,
        w_query,
        w_key,
        w_value,
        w_output,
        mixer_post_gain,
    )
    expert_out = expert_half(
        expert_input, expert_ids, route_weight, expert_gain, w_gate, w_up, w_down, expert_post_gain
    )
    return (mixer_out, expert_out)


def solution(mesh):
    placed = (
        P("ep", None),
        P("tp", None),
        P(),
        P(None, "tp"),
        P(None, "tp"),
        P(None, "tp"),
        P(),
        P(),
        P("ep", None),
        P("ep", None),
        P("ep", None),
        P(),
        P("ep", None, "tp"),
        P("ep", None, "tp"),
        P("ep", "tp", None),
        P(),
    )
    return jax.shard_map(
        per_device,
        mesh=mesh,
        in_specs=placed,
        out_specs=(P(("ep", "tp"), None), P(("ep", "tp"), None)),
        check_vma=False,
    )
```

profile of v0, /device:TPU:7, one launch (start us, length us, event | category | flops | bytes accessed | tf_op | source)
XLA Modules:
  0.0 430.0 jit_solution(15136423061495129708)
XLA Ops:
  8.1 2.2 fusion.29
  10.3 2.1 fusion.31
  12.4 0.8 fusion.42
  13.8 0.8 fusion.43
  14.6 0.7 pad_maximum_fusion
  16.4 29.5 %scatter_fusion = s32[4,8,32]{2,1,0:T(8,128)S(1)} fusion(s32[4,8,32]{2,1,0:T(8,128)S(1)} %broadcast_in_dim.39, s32[512]{0:T(512)S(1)} %fusion.50, s32[512]{0:T(512)S(1)} %fusion.52), kind=kCustom, calls=%fused_computation.2 | custom fusion | bytes 12288 | tf_op jit(solution)/shard_map/scatter | solution.py:147
  46.8 6.0 %gather_fusion = bf16[1024,2048]{1,0:T(8,128)(2,1)} fusion(bf16[257,2048]{1,0:T(8,128)(2,1)S(1)} %concatenate.10, s32[1024]{0:T(1024)S(1)} %broadcast_clamp_fusion), kind=kCustom, calls=%fused_computation | custom fusion | bytes 8392704 | tf_op jit(solution)/shard_map/gather | solution.py:153
  52.8 4.5 %copy.52 = bf16[4,8,32,2048]{3,1,0,2:T(8,128)(2,1)S(1)} copy(bf16[4,8,32,2048]{3,2,1,0:T(8,128)(2,1)} %bitcast.135) | data formatting | bytes 8388608 | tf_op jit(solution)/shard_map/gather | solution.py:153
  57.3 59.3 %all_to_all.26 = bf16[4,8,32,2048]{3,1,0,2:T(8,128)(2,1)S(1)} all-to-all(bf16[4,8,32,2048]{3,1,0,2:T(8,128)(2,1)S(1)} %copy.52), channel_id=1, replica_groups=mesh['ep'=32,'tp'=4] {'ep'}, dimensions={2} | all-to-all | bytes 8388608 | tf_op jit(solution)/shard_map/all_to_all | solution.py:154
  116.6 2.3 copy.53
  119.0 4.5 %fusion.33 = f32[1024,896]{1,0:T(8,128)S(1)} fusion(bf16[1024,2048]{1,0:T(8,128)(2,1)S(1)} %bitcast.138, bf16[1,2048,896]{2,1,0:T(8,128)(2,1)S(1)} %copy-done.12), kind=kOutput, calls=%fused_computation.42 | convolution fusion | flops 3758096384 | bytes 11534336 | tf_op jit(solution)/shard_map/dot_general | solution.py:157
  123.5 4.8 %multiply_convert_fusion = bf16[1024,896]{1,0:T(8,128)(2,1)S(1)} fusion(f32[1024,896]{1,0:T(8,128)S(1)} %fusion.33, bf16[1024,2048]{1,0:T(8,128)(2,1)S(1)} %bitcast.139, bf16[1,2048,896]{2,1,0:T(8,128)(2,1)S(1)} %copy-done.13), kind=kOutput, calls=%fused_computation.46 | convolution fusion | flops 3763601408 | bytes 13369344 | tf_op jit(solution)/shard_map/dot_general | solution.py:156
  128.3 6.1 %convolution_convert_fusion = bf16[4,8,32,2048]{3,2,1,0:T(8,128)(2,1)} fusion(bf16[4,8,32,896]{3,2,1,0:T(8,128)(2,1)S(1)} %bitcast.149, bf16[1,896,2048]{2,1,0:T(8,128)(2,1)S(1)} %copy-done.14), kind=kOutput, calls=%fused_computation.40 | convolution fusion | flops 3760193536 | bytes 9699328 | tf_op jit(solution)/shard_map/dot_general | solution.py:163
  134.4 0.6 copy-done.11
  135.2 0.7 dynamic-slice_bitcast_fusion.1
  136.0 0.8 convolution_convert_fusion.1
  136.8 2.6 fusion.60
  139.4 1.8 copy_bitcast_fusion
  141.3 54.4 %while.15 = (s32[]{:T(128)}, f32[1,4,512]{2,1,0:T(4,128)S(1)}, f32[1,4,512]{2,1,0:T(4,128)S(1)}, f32[1,4,512,64]{2,3,1,0:T(8,128)S(1)}, s32[32]{0:T(128)S(1)}, /...) while((s32[]{:T(128)}, f32[1,4,512]{2,1,0:T(4,128)S(1)}, ...), condition=%wide.region_6.7_spmd.clone, body=%wide.region_1.6_spmd.clone.sunk | while | flops 288889856 | bytes 15283061 | solution.py:110
  141.5 0.6 dynamic_slice.69
  142.8 6.4 %conditional.3 = ((f32[1,4,512]{2,1,0:T(4,128)S(1)}, f32[1,4,512]{2,1,0:T(4,128)S(1)}, f32[1,4,512,64]{2,3,1,0:T(8,128)S(1)})) conditional(s32[]{:T(128)} %convert_element_type.127, (f32[1,4,512]{2,1,0:T(4,128)S(1)}, f32[1,4,512]{2,1,0:T(4,128)S(1)}, f32[1,4,512,64]{2,3,1,0:T(8,128)S(1)}) %tuple.51, (s32[]{:T(128)}, s32[]{:T(128)}, ...), branch_computations={%region_2.2_spmd, %region_3.5_spmd} | conditional | flops 288889856 | bytes 15280722 | solution.py:108
  142.8 0.8 dynamic-slice_bitcast_fusion
  143.8 2.1 fusion.6
  145.9 1.7 fusion.14
  147.7 1.5 fusion.5
  149.2 0.6 dynamic_slice.69
  150.5 6.5 %conditional.3 = ((f32[1,4,512]{2,1,0:T(4,128)S(1)}, f32[1,4,512]{2,1,0:T(4,128)S(1)}, f32[1,4,512,64]{2,3,1,0:T(8,128)S(1)})) conditional(s32[]{:T(128)} %convert_element_type.127, (f32[1,4,512]{2,1,0:T(4,128)S(1)}, f32[1,4,512]{2,1,0:T(4,128)S(1)}, f32[1,4,512,64]{2,3,1,0:T(8,128)S(1)}) %tuple.51, (s32[]{:T(128)}, s32[]{:T(128)}, ...), branch_computations={%region_2.2_spmd, %region_3.5_spmd} | conditional | flops 288889856 | bytes 15280722 | solution.py:108
  150.5 0.8 dynamic-slice_bitcast_fusion
  151.5 2.1 fusion.6
  153.6 1.7 fusion.14
  155.4 1.5 fusion.5
  157.0 0.6 dynamic_slice.69
  158.3 0.6 dynamic_slice.69
  159.6 0.6 dynamic_slice.69
  171.2 0.6 dynamic_slice.69
  172.5 0.6 dynamic_slice.69
  195.8 0.7 copy.48
  196.5 4.2 all-to-all-start
  200.8 2.8 copy.54
  203.6 0.9 all-to-all-done
  204.5 196.3 %all-to-all-start.2 = ((bf16[8,32,2048]{2,0,1:T(8,128)(2,1)}), bf16[8,32,2048]{2,0,1:T(8,128)(2,1)S(1)}, u32[]{:S(2)}, u32[]{:S(2)}) async-start(bf16[8,32,2048]{2,0,1:T(8,128)(2,1)} %copy.54), calls=%async_computation.3 | async-start | bytes 2097152 | tf_op jit(solution)/shard_map/all_to_all | solution.py:175
  400.8 3.0 multiply_reduce_fusion.1
  403.8 1.0 multiply_convert_fusion.1
  404.8 13.1 %all-to-all-done.2 = bf16[8,32,2048]{2,0,1:T(8,128)(2,1)S(1)} async-done(((bf16[8,32,2048]{2,0,1:T(8,128)(2,1)}), bf16[8,32,2048]{2,0,1:T(8,128)(2,1)S(1)}, u32[]{:S(2)}, u32[]{:S(2)}) %all-to-all-start.2) | async-done | bytes 1048608 | tf_op jit(solution)/shard_map/all_to_all | solution.py:175
  418.4 0.9 gather_fusion.1
  419.4 0.7 reshape.259
  420.0 1.5 multiply_reduce_fusion
  421.7 0.8 multiply_convert_fusion.2
  (164 shorter events, 19.4 us)
Async XLA Ops:
  8.0 128.0 %copy-start = (bf16[2048,256]{1,0:T(8,128)(2,1)S(1)}, bf16[2048,256]{1,0:T(8,128)(2,1)}, u32[]{:S(2)}) copy-start(bf16[2048,256]{1,0:T(8,128)(2,1)} %param.23) | copy-start | bytes 3145732
  8.0 4.4 %copy-start.5 = (bf16[2048,64]{0,1:T(8,128)(2,1)S(1)}, bf16[2048,64]{0,1:T(8,128)(2,1)}, u32[]{:S(2)}) copy-start(bf16[2048,64]{0,1:T(8,128)(2,1)} %param.24) | copy-start | bytes 786436
  8.0 5.8 %copy-start.6 = (bf16[2048,64]{0,1:T(8,128)(2,1)S(1)}, bf16[2048,64]{0,1:T(8,128)(2,1)}, u32[]{:S(2)}) copy-start(bf16[2048,64]{0,1:T(8,128)(2,1)} %param.25) | copy-start | bytes 786436
  8.0 128.7 %all-gather.2.cloned.1.call-start = ((), (), s32[]{:S(2)}) async-start(), calls=%async_computation.4 | async-start | bytes 4325376 | tf_op jit(solution)/shard_map/all_gather | solution.py:18
  10.3 5.0 %copy-start.10 = (s32[256,2]{0,1:T(2,128)S(1)}, s32[256,2]{0,1:T(2,128)}, u32[]{:S(2)}) copy-start(s32[256,2]{0,1:T(2,128)} %param.29) | copy-start | bytes 6148
  12.4 1.4 copy-start.2
  13.8 32.3 %copy-start.4 = (bf16[256,2048]{1,0:T(8,128)(2,1)S(1)}, bf16[256,2048]{1,0:T(8,128)(2,1)}, u32[]{:S(2)}) copy-start(bf16[256,2048]{1,0:T(8,128)(2,1)} %param.28) | copy-start | bytes 3145732
  14.6 31.8 %copy-start.7 = (f32[2048]{0:T(1024)S(1)}, f32[2048]{0:T(1024)}, u32[]{:S(2)}) copy-start(f32[2048]{0:T(1024)} %param.31) | copy-start | bytes 24580
  15.3 185.5 %reduce-scatter.2.cloned.1.call-start = ((), (), s32[]{:S(2)}) async-start(), calls=%async_computation.5 | async-start | bytes 5242880 | tf_op jit(solution)/shard_map/reduce_scatter | solution.py:166
  116.6 2.4 copy-start.12
  119.0 4.5 %copy-start.13 = (bf16[1,2048,896]{2,1,0:T(8,128)(2,1)S(1)}, bf16[1,2048,896]{2,1,0:T(8,128)(2,1)}, u32[]{:S(2)}) copy-start(bf16[1,2048,896]{2,1,0:T(8,128)(2,1)} %param.32) | copy-start | bytes 11010052
  123.5 4.8 %copy-start.14 = (bf16[1,896,2048]{2,1,0:T(8,128)(2,1)S(1)}, bf16[1,896,2048]{2,1,0:T(8,128)(2,1)}, u32[]{:S(2)}) copy-start(bf16[1,896,2048]{2,1,0:T(8,128)(2,1)} %param.34) | copy-start | bytes 11010052
  134.4 0.7 copy-start.11
  134.4 1.6 copy-start.3
  196.5 7.9 %all-to-all-start = ((bf16[4,128,256]{1,2,0:T(8,128)(2,1)}), bf16[4,128,256]{1,2,0:T(8,128)(2,1)S(1)}, u32[]{:S(2)}, u32[]{:S(2)}) async-start(bf16[4,128,256]{1,2,0:T(8,128)(2,1)} %copy.48), calls=%async_computation | async-start | bytes 524288 | tf_op jit(solution)/shard_map/all_to_all | solution.py:119
  203.5 200.2 %copy-start.8 = (f32[2048]{0:T(1024)S(1)}, f32[2048]{0:T(1024)}, u32[]{:S(2)}) copy-start(f32[2048]{0:T(1024)} %param.27) | copy-start | bytes 24580
  204.5 213.4 %all-to-all-start.2 = ((bf16[8,32,2048]{2,0,1:T(8,128)(2,1)}), bf16[8,32,2048]{2,0,1:T(8,128)(2,1)S(1)}, u32[]{:S(2)}, u32[]{:S(2)}) async-start(bf16[8,32,2048]{2,0,1:T(8,128)(2,1)} %copy.54), calls=%async_computation.3 | async-start | bytes 2097152 | tf_op jit(solution)/shard_map/all_to_all | solution.py:175
  418.4 4.1 copy-start.1
  418.4 3.3 copy-start.9
Sparse Core Ops, SparseCore 0:
  15.4 51.4 all-gather.1
Sparse Core Ops, SparseCore 1:
  134.5 42.1 reduce-scatter.1
where the time goes:
time: 436 us; the launch traced here: 430 us
  starting transfers between devices  201 us (46%)
  local copies, waits for them, and re-layouts  75.8 us (17%)
  blocking collectives  59.3 us (14%)
  matrix products  28.3 us (6%)
  loops' own time  22.8 us (5%)
  between operations  15.9 us (4%)
  waiting for transfers between devices  14.1 us (3%)
  other arithmetic  13.4 us (3%)
    all_to_all x1, starting transfers between devices, expert_half(): lax.all_to_all(results, 'ep', split_axis=1, concat_axis=1, tiled=True)  196 us
    all_to_all x1, blocking collectives, expert_half(): lax.all_to_all(outgoing, 'ep', split_axis=2, concat_axis=2, tiled=True)  59.3 us
    scatter x1, local copies, waits for them, and re-layouts, expert_half(): slot_table = jnp.full((quarters, slot_count, experts), row_count, jnp.int...  29.5 us
    another operation x1, loops' own time, mixer_half(): lax.scan(one_block, running, (key_blocks, value_blocks, jnp.arange(block_...  22.3 us
    dynamic_slice x32, local copies, waits for them, and re-layouts, mixer_half(): lax.scan(one_block, running, (key_blocks, value_blocks, jnp.arange(block_...  18.8 us
    all_to_all x1, waiting for transfers between devices, expert_half(): lax.all_to_all(results, 'ep', split_axis=1, concat_axis=1, tiled=True)  13.1 us
    gather x2, local copies, waits for them, and re-layouts, expert_half(): outgoing = padded_rows[slot_table]  10.5 us
  transfers between devices with their start and end apart: 4, of which 2 were waited for; matrix products, arithmetic and copies ran while one was open for 24% of the time, Pallas kernels for 0%

commit v1 on v0

v1 whole, which is shorter than its diff:
```python
import functools
import math

import jax
import jax.numpy as jnp
from jax import lax
from jax.experimental import pallas as pl
from jax.experimental.pallas import tpu as pltpu
from jax.sharding import PartitionSpec as P

HD = 64
TOP_K = 2
NEG_FILL = -1e30
NORM_EPS = 1e-06
F32 = jnp.float32
BF16 = jnp.bfloat16


def norm_rows(values_in, gain_vec):
    widened = values_in.astype(F32)
    return (
        widened
        * lax.rsqrt(jnp.mean(widened * widened, axis=-1, keepdims=True) + NORM_EPS)
        * gain_vec
    )


def dot(a, b):
    return jnp.dot(a, b, preferred_element_type=F32)


def attention_kernel(n_ep, heads, half, kv_ref, g_ref, qt_ref, o_ref, qs, m_s, l_s, acc):
    me = lax.axis_index("ep")
    other = n_ep - 1 - me
    nq = heads * half
    row = lax.broadcasted_iota(jnp.int32, (128, nq), 0)
    col = lax.broadcasted_iota(jnp.int32, (128, nq), 1)
    sel = jnp.where((row < 3 * heads) & (row % heads == col // half), 1.0, 0.0).astype(BF16)
    zero = jnp.zeros((HD, nq), BF16)
    for hf in range(2):
        q = qt_ref[hf]
        qs[hf, 0] = jnp.concatenate([q, zero, sel], axis=0)
        qs[hf, 1] = jnp.concatenate([zero, q, sel], axis=0)
    m_s[...] = jnp.full(m_s.shape, NEG_FILL, F32)
    l_s[...] = jnp.zeros(l_s.shape, F32)
    acc[...] = jnp.zeros(acc.shape, F32)
    hidden = lax.broadcasted_iota(jnp.int32, (half, half), 0) > lax.broadcasted_iota(
        jnp.int32, (half, half), 1
    )

    def step(hf, kb, mode):
        kp = kv_ref[kb, 0:half, :]
        parts = [0] if mode == "first" else [0, 1]
        keys = [
            jnp.concatenate([kp, g_ref[kb, pt * half : (pt + 1) * half, :]], axis=1) for pt in parts
        ]
        vt = jnp.concatenate(
            [kv_ref[kb, half + HD * c : half + HD * (c + 1), :] for c in range(2 * len(parts))], axis=1
        )
        for h in range(heads):
            cols = slice(h * half, (h + 1) * half)
            sc = [dot(keys[pt], qs[hf, pt, :, cols]) for pt in parts]
            if mode != "full":
                sc[-1] = jnp.where(hidden, NEG_FILL, sc[-1])
            top = m_s[hf, 0:1, cols]
            new = top
            for s in sc:
                new = jnp.maximum(new, jnp.max(s, axis=0, keepdims=True))
            ps = [jnp.exp(s - new) for s in sc]
            factor = jnp.exp(top - new)
            den = l_s[hf, 0:1, cols] * factor
            for p in ps:
                den = den + jnp.sum(p, axis=0, keepdims=True)
            l_s[hf, 0:1, cols] = den
            m_s[hf, 0:1, cols] = new
            pb = jnp.concatenate([p.astype(BF16) for p in ps], axis=0)
            acc[hf, :, cols] = acc[hf, :, cols] * factor + dot(vt, pb)

    @pl.loop(0, me)
    def _(kb):
        step(0, kb, "full")

    step(0, me, "first")

    @pl.loop(0, other)
    def _(kb):
        step(1, kb, "full")

    step(1, other, "second")
    for hf in range(2):
        o_ref[hf] = (acc[hf] / l_s[hf, 0:1, :]).astype(BF16)


def attention(kv, gates, qt, n_ep, heads, half):
    nq = heads * half
    return pl.pallas_call(
        functools.partial(attention_kernel, n_ep, heads, half),
        out_shape=jax.ShapeDtypeStruct((2, HD, nq), BF16),
        in_specs=[pl.BlockSpec(memory_space=pltpu.VMEM)] * 3,
        out_specs=pl.BlockSpec(memory_space=pltpu.VMEM),
        scratch_shapes=[
            pltpu.VMEM((2, 2, 256, nq), BF16),
            pltpu.VMEM((2, 8, nq), F32),
            pltpu.VMEM((2, 8, nq), F32),
            pltpu.VMEM((2, HD, nq), F32),
        ],
        compiler_params=pltpu.CompilerParams(vmem_limit_bytes=48 * 1024 * 1024),
        cost_estimate=pl.CostEstimate(
            flops=30_000_000_000, bytes_accessed=9_000_000, transcendentals=17_000_000
        ),
        name="attention",
    )(kv, gates, qt)


def pieces_of(values):
    out, rest = [], values
    for _ in range(3):
        piece = lax.reduce_precision(rest, 8, 7)
        out.append(piece.astype(BF16))
        rest = rest - piece
    return out


def mixer_half(
    mixer_input, log_forget_total, mixer_gain, w_query, w_key, w_value, w_output, mixer_post_gain
):
    rows = mixer_input.shape[0]
    half = rows // 2
    heads = w_query.shape[1] // HD
    n_ep = lax.axis_size("ep")
    normed = norm_rows(mixer_input, mixer_gain).astype(BF16)
    queries = dot(normed, w_query).astype(BF16)
    keys = dot(normed, w_key).astype(BF16)
    values = dot(normed, w_value).astype(BF16)
    packed_keys = jnp.concatenate([keys[:half], keys[half:]], axis=1)
    values_t = values.T.reshape(HD, rows // 128, 128).transpose(1, 0, 2).reshape(half, 128)
    kv_own = jnp.concatenate([packed_keys, values_t], axis=0)
    kv = lax.all_gather(kv_own, "ep", axis=0, tiled=False)
    gates = jnp.concatenate(pieces_of(-log_forget_total), axis=0)
    gates = jnp.pad(gates.T, ((0, 0), (0, 128 - gates.shape[0]))).reshape(n_ep, rows, 128)
    swap = [(i, n_ep - 1 - i) for i in range(n_ep)]
    qt = (queries * BF16(HD**-0.5)).reshape(2, half, heads, HD).transpose(0, 3, 2, 1)
    qt = qt.reshape(2, HD, heads * half)
    far = lax.ppermute(qt[1], "ep", swap)
    out = attention(kv, gates, jnp.stack([qt[0], far]), n_ep, heads, half)
    far_out = lax.ppermute(out[1], "ep", swap)
    mixed = jnp.stack([out[0], far_out]).reshape(2, HD, heads, half)
    mixed_heads = mixed.transpose(0, 3, 2, 1).reshape(rows, heads * HD)
    by_rows = lax.all_to_all(mixed_heads, "tp", split_axis=0, concat_axis=1, tiled=True)
    projected = dot(by_rows, w_output)
    return norm_rows(projected, mixer_post_gain).astype(BF16)


def expert_half(
    expert_input, expert_ids, route_weight, expert_gain, w_gate, w_up, w_down, expert_post_gain
):
    row_count, width = expert_input.shape
    quarters = lax.axis_size("tp")
    experts = lax.axis_size("ep")
    quarter_rows = row_count // quarters
    slots = 2 * TOP_K * quarter_rows // experts
    own_quarter = lax.axis_index("tp")
    normed = norm_rows(expert_input, expert_gain).astype(BF16)
    ids = expert_ids.reshape(quarters, quarter_rows, TOP_K)
    each = jnp.arange(experts, dtype=jnp.int32)
    chosen = jnp.any(ids[..., None] == each, axis=2)
    before = jnp.tril(jnp.ones((quarter_rows, quarter_rows), BF16), -1)
    ranks = jnp.einsum(
        "ut,bte->bue", before, chosen.astype(BF16), preferred_element_type=F32
    ).astype(jnp.int32)
    ranks = jnp.where(chosen, ranks, -1)
    table = (ranks[..., None] == jnp.arange(slots, dtype=jnp.int32)).astype(BF16)
    table = table.reshape(quarters, quarter_rows, experts * slots)
    outgoing = jnp.einsum(
        "bts,btd->bsd",
        table,
        normed.reshape(quarters, quarter_rows, width),
        preferred_element_type=F32,
    ).astype(BF16)
    outgoing = outgoing.reshape(quarters, experts, slots, width)
    arrived = lax.all_to_all(outgoing, "ep", split_axis=1, concat_axis=1, tiled=True)
    flat_rows = arrived.reshape(-1, width)
    gate_part = dot(flat_rows, w_gate[0])
    up_part = dot(flat_rows, w_up[0])
    hidden = (jax.nn.silu(gate_part) * up_part).astype(BF16)
    product = dot(hidden, w_down[0]).astype(BF16)
    summed = lax.psum_scatter(
        product.reshape(quarters, experts, slots, width), "tp", scatter_dimension=0, tiled=True
    )
    returned = lax.all_to_all(summed[0], "ep", split_axis=0, concat_axis=0, tiled=True)
    flat_results = returned.reshape(experts * slots, width)
    own_table = lax.dynamic_index_in_dim(table, own_quarter, 0, keepdims=False)
    own_table = own_table.reshape(quarter_rows, experts, slots)
    own_ids = lax.dynamic_index_in_dim(ids, own_quarter, 0, keepdims=False)
    own_weights = lax.dynamic_slice_in_dim(
        route_weight, own_quarter * quarter_rows, quarter_rows, 0
    )
    combined = jnp.zeros((quarter_rows, width), F32)
    for k in range(TOP_K):
        mine = (own_ids[:, k, None] == each).astype(BF16)[:, :, None]
        picked = dot((own_table * mine).reshape(quarter_rows, -1), flat_results)
        combined = combined + own_weights[:, k, None] * picked
    return norm_rows(combined, expert_post_gain).astype(BF16)


def per_device(*args):
    return (mixer_half(*args[:8]), expert_half(*args[8:]))


def solution(mesh):
    placed = (
        P("ep", None),
        P("tp", None),
        P(),
        P(None, "tp"),
        P(None, "tp"),
        P(None, "tp"),
        P(),
        P(),
        P("ep", None),
        P("ep", None),
        P("ep", None),
        P(),
        P("ep", None, "tp"),
        P("ep", None, "tp"),
        P("ep", "tp", None),
        P(),
    )
    return jax.shard_map(
        per_device,
        mesh=mesh,
        in_specs=placed,
        out_specs=(P(("ep", "tp"), None), P(("ep", "tp"), None)),
        check_vma=False,
    )
```

time: 436 us -> 232 us (0.53)
  starting transfers between devices: 201 us -> 25.6 us
  blocking collectives: 59.3 us -> 0 us
  waiting for transfers between devices: 14.1 us -> 72.2 us
  Pallas kernels: 0 us -> 55.1 us
  local copies, waits for them, and re-layouts: 75.8 us -> 25.5 us
  loops' own time: 22.8 us -> 0 us
    all_to_all x1 -> x2, starting transfers between devices: 196 us -> 14.2 us  [the longest x1 8.83 us: expert_half(): lax.all_to_all(outgoing, 'ep', split_axis=1, concat_axis=1, tiled=True)]
    all_to_all x1 -> x0, blocking collectives: 59.3 us -> none  [expert_half(): lax.all_to_all(outgoing, 'ep', split_axis=2, concat_axis=2, tiled=True)]
    pallas_call x0 -> x1, Pallas kernels: none -> 55.1 us  [attention(): pl.pallas_call(functools.partial(attention_kernel, n_ep, heads, half), ou...]
    all_to_all x1 -> x2, waiting for transfers between devices: 13.1 us -> 61.4 us  [the longest x1 48.3 us: expert_half(): lax.all_to_all(outgoing, 'ep', split_axis=1, concat_axis=1, tiled=True)]
    scatter x1 -> x0, local copies, waits for them, and re-layouts: 29.5 us -> none  [expert_half(): slot_table = jnp.full((quarters, slot_count, experts), row_count, jnp.int...]
    another operation x33 -> x0, loops' own time: 22.8 us -> none  [the longest x1 22.3 us: mixer_half(): lax.scan(one_block, running, (key_blocks, value_blocks, jnp.arange(block_...]
    dynamic_slice x33 -> x0, local copies, waits for them, and re-layouts: 19.5 us -> none  [the longest x32 18.8 us: mixer_half(): lax.scan(one_block, running, (key_blocks, value_blocks, jnp.arange(block_...]
    gather x3 -> x0, local copies, waits for them, and re-layouts: 11.4 us -> none  [the longest x2 10.5 us: expert_half(): outgoing = padded_rows[slot_table]]
  transfers between devices with their start and end apart: 4 -> 7, of which waited for: 2 -> 4; matrix products, arithmetic and copies ran while one was open for 24% -> 21% of each run, Pallas kernels for 0% -> 24%
where the time goes in v1:
time: 232 us; the launch traced here: 229 us
  waiting for transfers between devices  72.2 us (31%)
  Pallas kernels  55.1 us (24%)
  starting transfers between devices  25.6 us (11%)
  local copies, waits for them, and re-layouts  25.5 us (11%)
  matrix products  24 us (10%)
  between operations  15.9 us (7%)
  other arithmetic  11 us (5%)
    pallas_call x1, Pallas kernels, attention(): pl.pallas_call(functools.partial(attention_kernel, n_ep, heads, half), ou...  55.1 us
    all_to_all x1, waiting for transfers between devices, expert_half(): lax.all_to_all(outgoing, 'ep', split_axis=1, concat_axis=1, tiled=True)  48.3 us
    dot_general x9, matrix products, dot(): return jnp.dot(a, b, preferred_element_type=F32)  22.5 us
    all_to_all x1, waiting for transfers between devices, expert_half(): lax.all_to_all(summed[0], 'ep', split_axis=0, concat_axis=0, tiled=True)  13.1 us
    all_to_all x1, starting transfers between devices, expert_half(): lax.all_to_all(outgoing, 'ep', split_axis=1, concat_axis=1, tiled=True)  8.83 us
    unnamed x28, local copies, waits for them, and re-layouts  7.15 us
    ppermute x1, waiting for transfers between devices, mixer_half(): far_out = lax.ppermute(out[1], 'ep', swap)  6.59 us
    all_gather x1, local copies, waits for them, and re-layouts, mixer_half(): kv = lax.all_gather(kv_own, 'ep', axis=0, tiled=False)  6.41 us
  transfers between devices with their start and end apart: 7, of which 4 were waited for; matrix products, arithmetic and copies ran while one was open for 21% of the time, Pallas kernels for 24%

profile of v1, /device:TPU:7, one launch (start us, length us, event | category | flops | bytes accessed | tf_op | source)
XLA Modules:
  0.0 229.3 jit_solution(2691858422700017915)
XLA Ops:
  8.1 2.2 fusion
  10.3 2.1 fusion.2
  12.4 0.8 fusion.19
  13.3 1.7 convolution_convert_fusion.3
  15.1 0.7 pad_maximum_fusion.1
  15.8 1.5 fusion.13
  17.5 0.2 fusion.18
  17.7 1.5 fusion.15
  19.3 1.3 convert_bitcast_fusion
  20.6 2.3 copy.88
  22.8 8.8 %all-to-all-start.1 = ((bf16[4,32,8,2048]{3,2,0,1:T(8,128)(2,1)}), bf16[4,32,8,2048]{3,2,0,1:T(8,128)(2,1)}, u32[]{:S(2)}, u32[]{:S(2)}) async-start(bf16[4,32,8,2048]{3,2,0,1:T(8,128)(2,1)} %copy.88), calls=%async_computation.1 | async-start | bytes 8388608 | tf_op jit(solution)/shard_map/all_to_all | solution.py:181
  31.7 0.7 fusion.16
  32.5 0.1 copy.79
  32.7 0.4 fusion.43
  33.1 0.2 copy.81
  33.3 5.3 %collective-permute-start = (bf16[64,1024]{1,0:T(8,128)(2,1)S(1)}, bf16[64,1024]{1,0:T(8,128)(2,1)S(1)}, u32[]{:S(2)}, u32[]{:S(2)}) collective-permute-start(bf16[64,1024]{1,0:T(8,128)(2,1)S(1)} %bitcast.114), channel_id=1, source_target_pairs={{0,124},{4,120},{8,116},{12,112},{16,108},{20,104},{24,100},{28,96... | collective-permute-start | bytes 393224 | tf_op jit(solution)/shard_map/ppermute | solution.py:144
  38.6 48.3 %all-to-all-done.1 = bf16[4,32,8,2048]{3,2,0,1:T(8,128)(2,1)} async-done(((bf16[4,32,8,2048]{3,2,0,1:T(8,128)(2,1)}), bf16[4,32,8,2048]{3,2,0,1:T(8,128)(2,1)}, u32[]{:S(2)}, u32[]{:S(2)}) %all-to-all-start.1) | async-done | bytes 4194336 | tf_op jit(solution)/shard_map/all_to_all | solution.py:181
  86.9 2.7 %copy.89 = bf16[4,32,8,2048]{3,2,1,0:T(8,128)(2,1)S(1)} copy(bf16[4,32,8,2048]{3,2,0,1:T(8,128)(2,1)} %all-to-all-done.1) | data formatting | bytes 8388608 | tf_op jit(solution)/shard_map/all_to_all | solution.py:181
  89.5 0.6 copy-done.10
  90.2 4.5 %fusion.4 = f32[1024,896]{1,0:T(8,128)S(1)} fusion(bf16[1024,2048]{1,0:T(8,128)(2,1)S(1)} %bitcast.106, bf16[1,2048,896]{2,1,0:T(8,128)(2,1)S(1)} %copy-done.10), kind=kOutput, calls=%fused_computation.8 | convolution fusion | flops 3758096384 | bytes 11534336 | tf_op jit(solution)/shard_map/dot_general | solution.py:29
  94.7 4.8 %multiply_convert_fusion = bf16[1024,896]{1,0:T(8,128)(2,1)S(1)} fusion(f32[1024,896]{1,0:T(8,128)S(1)} %fusion.4, bf16[1024,2048]{1,0:T(8,128)(2,1)S(1)} %bitcast.107, bf16[1,2048,896]{2,1,0:T(8,128)(2,1)S(1)} %copy-done.11), kind=kOutput, calls=%fused_computation.12 | convolution fusion | flops 3763601408 | bytes 13369344 | tf_op jit(solution)/shard_map/dot_general | solution.py:29
  99.5 6.1 %convolution_convert_fusion = bf16[1024,2048]{1,0:T(8,128)(2,1)} fusion(bf16[1024,896]{1,0:T(8,128)(2,1)S(1)} %multiply_convert_fusion, bf16[1,896,2048]{2,1,0:T(8,128)(2,1)S(1)} %copy-done.12), kind=kOutput, calls=%fused_computation.6 | convolution fusion | flops 3760193536 | bytes 9699328 | tf_op jit(solution)/shard_map/dot_general | solution.py:29
  105.7 0.9 copy-done.4
  106.6 0.1 reduce-precision_convert_fusion.1
  106.7 0.2 maximum_bitcast_fusion
  107.0 3.3 %copy.91 = bf16[16384,12]{1,0:T(8,128)(2,1)} copy(bf16[16384,12]{0,1:T(8,128)(2,1)S(1)} %maximum_bitcast_fusion) | data formatting | bytes 786432
  110.3 0.2 copy.80
  110.5 4.2 %pad.4.clone = bf16[16384,128]{1,0:T(8,128)(2,1)} pad(bf16[16384,12]{1,0:T(8,128)(2,1)} %copy.91, bf16[]{:T(256)} %constant.17.clone.1), padding=0_0x0_116 | pad | bytes 4587522 | tf_op jit(solution)/shard_map/jit(_pad)/pad | solution.py:140
  114.7 0.1 bitcast_compare_fusion
  114.9 6.4 %copy.77 = bf16[16384,128]{1,0:T(8,128)(2,1)} copy(bf16[16384,128]{0,1:T(8,128)(2,1)} %all-gather.3.cloned.1.call-done) | data formatting | bytes 8388608 | tf_op jit(solution)/shard_map/all_gather | solution.py:138
  121.4 2.2 copy-done.2
  123.6 55.1 %attention.1 = bf16[2,64,1024]{2,1,0:T(8,128)(2,1)S(1)} custom-call(bf16[32,512,128]{2,1,0:T(8,128)(2,1)S(1)} %bitcast.103, bf16[32,512,128]{2,1,0:T(8,128)(2,1)} %bitcast.105, bf16[2,64,1024]{2,1,0:T(8,128)(2,1)S(1)} %pad_maximum_fusion.qt_ref), custom_call_target="tpu_custom_call" | custom-call | flops 30000001024 | bytes 9000000 | tf_op jit(solution)/shard_map/attention/pallas_call | solution.py:96
  178.7 1.9 collective-permute-start.1
  180.8 0.2 copy.82
  181.0 6.6 %collective-permute-done.1 = bf16[64,1024]{1,0:T(8,128)(2,1)S(1)} collective-permute-done((bf16[64,1024]{1,0:T(8,128)(2,1)S(1)}, bf16[64,1024]{1,0:T(8,128)(2,1)S(1)}, u32[]{:S(2)}, u32[]{:S(2)}) %collective-permute-start.1) | collective-permute-done | bytes 131104 | tf_op jit(solution)/shard_map/ppermute | solution.py:146
  187.6 0.2 copy.83
  187.9 0.5 maximum_bitcast_fusion.1
  188.4 0.2 all_to_all.20
  188.6 0.7 copy.84
  189.3 4.2 %all-to-all-start = ((bf16[4,128,256]{1,2,0:T(8,128)(2,1)}), bf16[4,128,256]{1,2,0:T(8,128)(2,1)S(1)}, u32[]{:S(2)}, u32[]{:S(2)}) async-start(bf16[4,128,256]{1,2,0:T(8,128)(2,1)} %copy.84), calls=%async_computation | async-start | bytes 524288 | tf_op jit(solution)/shard_map/all_to_all | solution.py:149
  193.5 4.2 %all-to-all-done = bf16[4,128,256]{1,2,0:T(8,128)(2,1)S(1)} async-done(((bf16[4,128,256]{1,2,0:T(8,128)(2,1)}), bf16[4,128,256]{1,2,0:T(8,128)(2,1)S(1)}, u32[]{:S(2)}, u32[]{:S(2)}) %all-to-all-start) | async-done | bytes 262176 | tf_op jit(solution)/shard_map/all_to_all | solution.py:149
  197.7 5.4 %all-to-all-start.2 = ((bf16[32,8,2048]{2,1,0:T(8,128)(2,1)}), bf16[32,8,2048]{2,1,0:T(8,128)(2,1)S(1)}, u32[]{:S(2)}, u32[]{:S(2)}) async-start(bf16[32,8,2048]{2,1,0:T(8,128)(2,1)} %bitcast.111), calls=%async_computation.3 | async-start | bytes 2097152 | tf_op jit(solution)/shard_map/all_to_all | solution.py:190
  203.1 3.1 %multiply_reduce_fusion = (f32[128]{0:T(128)S(1)}, f32[128,2048]{1,0:T(8,128)S(1)}) fusion(bf16[128,1024]{0,1:T(8,128)(2,1)S(1)} %bitcast.110, bf16[1024,2048]{1,0:T(8,128)(2,1)} %param.22), kind=kOutput, calls=%fused_computation.32 | convolution fusion | flops 537395072 | bytes 5505536 | tf_op jit(solution)/shard_map/dot_general | solution.py:29
  206.2 1.0 multiply_convert_fusion.1
  207.1 13.1 %all-to-all-done.2 = bf16[32,8,2048]{2,1,0:T(8,128)(2,1)S(1)} async-done(((bf16[32,8,2048]{2,1,0:T(8,128)(2,1)}), bf16[32,8,2048]{2,1,0:T(8,128)(2,1)S(1)}, u32[]{:S(2)}, u32[]{:S(2)}) %all-to-all-start.2) | async-done | bytes 1048608 | tf_op jit(solution)/shard_map/all_to_all | solution.py:190
  220.2 0.3 fusion.12
  220.6 0.4 multiply_reduce_fusion.1
  221.0 0.8 multiply_convert_fusion.2
  (55 shorter events, 1.0 us)
Async XLA Ops:
  8.0 23.7 %copy-start = (bf16[2048,256]{1,0:T(8,128)(2,1)S(1)}, bf16[2048,256]{1,0:T(8,128)(2,1)}, u32[]{:S(2)}) copy-start(bf16[2048,256]{1,0:T(8,128)(2,1)} %param.19) | copy-start | bytes 3145732
  8.0 4.4 %copy-start.3 = (bf16[2048,64]{0,1:T(8,128)(2,1)S(1)}, bf16[2048,64]{0,1:T(8,128)(2,1)}, u32[]{:S(2)}) copy-start(bf16[2048,64]{0,1:T(8,128)(2,1)} %param.21) | copy-start | bytes 786436
  8.0 106.9 %all-gather.3.cloned.1.call-start = ((), (), s32[]{:S(2)}) async-start(), calls=%async_computation.5 | async-start | bytes 4325376 | tf_op jit(solution)/shard_map/all_gather | solution.py:138
  12.4 4.9 %copy-start.8 = (s32[256,2]{0,1:T(2,128)S(1)}, s32[256,2]{0,1:T(2,128)}, u32[]{:S(2)}) copy-start(s32[256,2]{0,1:T(2,128)} %param.25) | copy-start | bytes 6148
  12.4 5.3 %copy-start.5 = (f32[2048]{0:T(1024)S(1)}, f32[2048]{0:T(1024)}, u32[]{:S(2)}) copy-start(f32[2048]{0:T(1024)} %param.27) | copy-start | bytes 24580
  22.8 64.0 %all-to-all-start.1 = ((bf16[4,32,8,2048]{3,2,0,1:T(8,128)(2,1)}), bf16[4,32,8,2048]{3,2,0,1:T(8,128)(2,1)}, u32[]{:S(2)}, u32[]{:S(2)}) async-start(bf16[4,32,8,2048]{3,2,0,1:T(8,128)(2,1)} %copy.88), calls=%async_computation.1 | async-start | bytes 8388608 | tf_op jit(solution)/shard_map/all_to_all | solution.py:181
  31.7 166.0 %reduce-scatter.2.cloned.1.call-start = ((), (), s32[]{:S(2)}) async-start(), calls=%async_computation.4 | async-start | bytes 5242880 | tf_op jit(solution)/shard_map/reduce_scatter | solution.py:187
  33.3 81.6 %collective-permute-start = (bf16[64,1024]{1,0:T(8,128)(2,1)S(1)}, bf16[64,1024]{1,0:T(8,128)(2,1)S(1)}, u32[]{:S(2)}, u32[]{:S(2)}) collective-permute-start(bf16[64,1024]{1,0:T(8,128)(2,1)S(1)} %bitcast.114), channel_id=1, source_target_pairs={{0,124},{4,120},{8,116},{12,112},{16,108},{20,104},{24,100},{28,96... | collective-permute-start | bytes 393224 | tf_op jit(solution)/shard_map/ppermute | solution.py:144
  86.9 3.3 %copy-start.10 = (bf16[1,2048,896]{2,1,0:T(8,128)(2,1)S(1)}, bf16[1,2048,896]{2,1,0:T(8,128)(2,1)}, u32[]{:S(2)}) copy-start(bf16[1,2048,896]{2,1,0:T(8,128)(2,1)} %param.29) | copy-start | bytes 11010052
  90.2 4.5 %copy-start.11 = (bf16[1,2048,896]{2,1,0:T(8,128)(2,1)S(1)}, bf16[1,2048,896]{2,1,0:T(8,128)(2,1)}, u32[]{:S(2)}) copy-start(bf16[1,2048,896]{2,1,0:T(8,128)(2,1)} %param.28) | copy-start | bytes 11010052
  94.7 4.8 %copy-start.12 = (bf16[1,896,2048]{2,1,0:T(8,128)(2,1)S(1)}, bf16[1,896,2048]{2,1,0:T(8,128)(2,1)}, u32[]{:S(2)}) copy-start(bf16[1,896,2048]{2,1,0:T(8,128)(2,1)} %param.30) | copy-start | bytes 11010052
  105.6 0.9 copy-start.4
  121.4 2.2 copy-start.2
  123.6 57.1 %copy-start.9 = (f32[256,2]{0,1:T(2,128)S(1)}, f32[256,2]{0,1:T(2,128)}, u32[]{:S(2)}) copy-start(f32[256,2]{0,1:T(2,128)} %param.26) | copy-start | bytes 6148
  178.7 8.9 %collective-permute-start.1 = (bf16[64,1024]{1,0:T(8,128)(2,1)S(1)}, bf16[64,1024]{1,0:T(8,128)(2,1)S(1)}, u32[]{:S(2)}, u32[]{:S(2)}) collective-permute-start(bf16[64,1024]{1,0:T(8,128)(2,1)S(1)} %get-tuple-element.3), channel_id=1, source_target_pairs={{0,124},{4,120},{8,116},{12,112},{16,108},{20,104},{24,100},{28,96... | collective-permute-start | bytes 393224 | tf_op jit(solution)/shard_map/ppermute | solution.py:146
  189.3 8.3 %all-to-all-start = ((bf16[4,128,256]{1,2,0:T(8,128)(2,1)}), bf16[4,128,256]{1,2,0:T(8,128)(2,1)S(1)}, u32[]{:S(2)}, u32[]{:S(2)}) async-start(bf16[4,128,256]{1,2,0:T(8,128)(2,1)} %copy.84), calls=%async_computation | async-start | bytes 524288 | tf_op jit(solution)/shard_map/all_to_all | solution.py:149
  197.7 8.5 %copy-start.6 = (f32[2048]{0:T(1024)S(1)}, f32[2048]{0:T(1024)}, u32[]{:S(2)}) copy-start(f32[2048]{0:T(1024)} %param.23) | copy-start | bytes 24580
  197.7 22.5 %all-to-all-start.2 = ((bf16[32,8,2048]{2,1,0:T(8,128)(2,1)}), bf16[32,8,2048]{2,1,0:T(8,128)(2,1)S(1)}, u32[]{:S(2)}, u32[]{:S(2)}) async-start(bf16[32,8,2048]{2,1,0:T(8,128)(2,1)} %bitcast.111), calls=%async_computation.3 | async-start | bytes 2097152 | tf_op jit(solution)/shard_map/all_to_all | solution.py:190
  203.1 18.8 %copy-start.1 = (bf16[2048,256]{1,0:T(8,128)(2,1)S(1)}, bf16[2048,256]{1,0:T(8,128)(2,1)}, u32[]{:S(2)}) copy-start(bf16[2048,256]{1,0:T(8,128)(2,1)} %param.19) | copy-start | bytes 3145732
  206.2 14.9 %copy-start.7 = (f32[2048]{0:T(1024)S(1)}, f32[2048]{0:T(1024)}, u32[]{:S(2)}) copy-start(f32[2048]{0:T(1024)} %param.31) | copy-start | bytes 24580
Sparse Core Ops, SparseCore 0:
  15.9 83.1 all-gather.2
Sparse Core Ops, SparseCore 1:
  105.7 43.7 reduce-scatter.1

commit v2 on v1

v2 whole, which is shorter than its diff:
```python
import functools

import jax
import jax.numpy as jnp
from jax import lax
from jax.experimental import pallas as pl
from jax.experimental.pallas import tpu as pltpu
from jax.sharding import PartitionSpec as P

HD = 64
TOP_K = 2
NEG_FILL = -1e30
NORM_EPS = 1e-06
F32 = jnp.float32
BF16 = jnp.bfloat16
SLOT = 8


def norm_rows(values_in, gain_vec):
    widened = values_in.astype(F32)
    return (
        widened
        * lax.rsqrt(jnp.mean(widened * widened, axis=-1, keepdims=True) + NORM_EPS)
        * gain_vec
    )


def dot(a, b):
    return jnp.dot(a, b, preferred_element_type=F32)


def dot_t(a, b):
    return lax.dot_general(a, b, (((0,), (0,)), ((), ())), preferred_element_type=F32)


def iota(shape, dim):
    return lax.broadcasted_iota(jnp.int32, shape, dim)


def whole_kernel(
    x_ref, lf_ref, again_ref, wq_ref, wk_ref, wv_ref, wo_hbm, apost_ref,
    m_ref, ids_ref, rw_ref, mgain_ref, wg_hbm, wu_hbm, wd_hbm, mpost_ref,
    mix_out, exp_out,
    wg, wu, wd, wo, w_sem,
    outgoing, arr, prod, own, far_s, far_r, near_s, near_r, res, ret,
    kv, qo, qf, gs, qs, m_s, acc, s_a, s_b, ob, mx,
    disp_ss, disp_rs, fwd_ss, fwd_rs, far_ss, far_rs, near_ss, near_rs, ret_ss, ret_rs,
    q_sem, k1_ss, k1_rs, k2_ss, k2_rs, k3_ss, k3_rs, ob_ss, ob_rs,
):
    me = lax.axis_index("ep")
    p = lax.axis_index("tp")
    z, y, c = me // 8, (me // 2) % 4, me % 2
    mirror = 31 - me
    parity = p % 2
    rows = x_ref.shape[0]
    half = rows // 2
    heads = wq_ref.shape[1] // HD
    nq = heads * half
    width = x_ref.shape[1]
    tokens = m_ref.shape[0]
    quarter = tokens // 4
    experts = arr.shape[1]
    upper = experts // 2

    def ep_of(a, b, d):
        return ((a + 8) % 4) * 8 + ((b + 8) % 4) * 2 + (d + 2) % 2

    def away(r, sign):
        g, j, d = r // 8, (r // 2) % 4, r % 2
        return ep_of(z + sign * j, y + sign * (g + j), c + d)

    def send(src, dst, s_sem, r_sem, ep, tp):
        return pltpu.make_async_remote_copy(
            src_ref=src,
            dst_ref=dst,
            send_sem=s_sem,
            recv_sem=r_sem,
            device_id={"ep": ep, "tp": tp},
            device_id_type=pl.DeviceIdType.MESH,
        )

    weights = [
        pltpu.make_async_copy(a, b, w_sem.at[k])
        for k, (a, b) in enumerate(((wg_hbm.at[0], wg), (wu_hbm.at[0], wu), (wd_hbm.at[0], wd), (wo_hbm, wo)))
    ]
    for w in weights:
        w.start()

    normed_m = norm_rows(m_ref[...], mgain_ref[...]).astype(BF16)
    each = iota((tokens, experts), 1)
    chosen = ((ids_ref[:, 0:1] == each) | (ids_ref[:, 1:2] == each)).astype(F32).astype(BF16)
    t_row, t_col = iota((tokens, tokens), 0), iota((tokens, tokens), 1)
    before = ((t_row // quarter == t_col // quarter) & (t_row < t_col)).astype(F32).astype(BF16)
    same = (t_row == t_col).astype(F32).astype(BF16)
    chosen_t = dot_t(chosen, same)
    ranks_t = dot_t(chosen, before)
    ranks_t = jnp.where(chosen_t > 0.5, ranks_t, -1.0)
    block_of = iota((experts, tokens), 1) // quarter
    for hb in range(2):
        mine = jnp.where(block_of == parity + 2 * hb, ranks_t, -1.0)
        wide = jnp.broadcast_to(mine[:, None, :], (experts, SLOT, tokens))
        table = jnp.where(wide == iota((experts, SLOT, tokens), 1).astype(F32), 1.0, 0.0)
        table = table.reshape(experts * SLOT, tokens).astype(BF16)
        picked = dot(table, normed_m)
        outgoing[:, hb] = picked.reshape(experts, SLOT, width).astype(BF16)

    def disp(r, peer):
        return send(outgoing.at[peer], arr.at[0, r], disp_ss.at[r], disp_rs.at[r], peer, p)

    def fwd(r):
        return send(
            arr.at[0, r], arr.at[1, r], fwd_ss.at[r], fwd_rs.at[r], me, (p + 1 + 2 * (r % 2)) % 4
        )

    @pl.loop(1, experts)
    def _(r):
        disp(r, away(r, 1)).start()

    arr[0, 0] = outgoing[me]

    normed_a = norm_rows(x_ref[...], again_ref[...]).astype(BF16)
    kt = dot(normed_a, wk_ref[...]).astype(BF16).astype(F32)
    vt = dot(normed_a, wv_ref[...]).astype(BF16).astype(F32)
    kv[me] = jnp.transpose(jnp.concatenate([kt, vt], axis=1)).astype(BF16)
    qt = dot(normed_a, wq_ref[...]).astype(BF16).astype(F32) * (HD**-0.5)
    qt = jnp.transpose(qt).astype(BF16)
    for hf in range(2):
        for h in range(heads):
            qo[hf, :, h * half : (h + 1) * half] = qt[
                h * HD : (h + 1) * HD, hf * half : (hf + 1) * half
            ]
    swap = send(qo.at[1], qf, q_sem.at[0], q_sem.at[1], mirror, p)
    swap.start()

    def first(part, d):
        ref = kv.at[me, part * HD : (part + 1) * HD]
        to = ep_of(z + d, y, c) if part == 0 else ep_of(z, y + d, c)
        return send(ref, ref, k1_ss.at[part, d], k1_rs.at[part, d], to, p)

    def second(part, a, d):
        owner = ep_of(z - a, y, c) if part == 0 else ep_of(z, y - a, c)
        to = ep_of(z, y + d, c) if part == 0 else ep_of(z + d, y, c)
        ref = kv.at[owner, part * HD : (part + 1) * HD]
        return send(ref, ref, k2_ss.at[part, a, d], k2_rs.at[part, a, d], to, p)

    def third(k):
        ref = kv.at[ep_of(z - k // 4, y - k % 4, c)]
        return send(ref, ref, k3_ss.at[k], k3_rs.at[k], ep_of(z, y, c + 1), p)

    for part in range(2):
        for d in range(1, 4):
            first(part, d).start()

    @pl.loop(0, experts)
    def _(kb):
        rest = -lf_ref[:, pl.ds(pl.multiple_of(kb * rows, rows), rows)]
        for k in range(3):
            piece = rest.astype(BF16).astype(F32)
            gs[kb, k * heads : (k + 1) * heads, :] = piece
            rest = rest - piece
        gs[kb, 3 * heads : 16, :] = jnp.zeros((16 - 3 * heads, rows), F32)

    fwd(0).start()

    @pl.loop(1, experts)
    def _(r):
        disp(r, away(r, 1)).wait_recv()
        fwd(r).start()

    for w in weights[:3]:
        w.wait()

    def ffn(v, u):
        rows_in = arr[v, pl.ds(u * upper, upper)].reshape(upper * 2 * SLOT, width)
        gate = dot(rows_in, wg[...])
        up = dot(rows_in, wu[...])
        hidden = (gate / (1.0 + jnp.exp(-gate)) * up).astype(BF16)
        tile = 512

        for n in range(width // tile):
            prod[:, :, :, n * tile : (n + 1) * tile] = dot(
                hidden, wd[:, n * tile : (n + 1) * tile]
            ).reshape(upper, 2, SLOT, tile)

    def far(u):
        return send(
            far_s.at[u], far_r.at[u], far_ss.at[u], far_rs.at[u], me, (p + 1 + 2 * u) % 4
        )

    @pl.loop(0, 2)
    def _(u):
        ffn(0, u)
        own[pl.ds(u * upper, upper)] = prod[:, p // 2].astype(BF16)
        far_s[u] = prod[:, 1 - p // 2].astype(BF16)
        far(u).start()

    for part in range(2):
        for a in range(4):
            if a > 0:
                first(part, a).wait_recv()
            for d in range(1, 4):
                second(part, a, d).start()

    plus = ((p + 1) % 4) // 2

    def near(u, k):
        side = (u + k) % 2
        return send(
            near_s.at[u, k],
            near_r.at[side, pl.ds(u * upper, upper)],
            near_ss.at[u, side],
            near_rs.at[u, side],
            me,
            (p + 1 + 2 * side) % 4,
        )

    @pl.loop(0, 2)
    def _(u):
        @pl.loop(0, upper)
        def _(k):
            fwd(u * upper + k).wait_recv()

        ffn(1, u)
        far(u).wait_recv()
        joined = (plus + u) % 2
        near_s[u, 0] = (
            prod[:, joined].astype(BF16).astype(F32) + far_r[u].astype(F32)
        ).astype(BF16)
        near_s[u, 1] = prod[:, 1 - joined].astype(BF16)
        near(u, 0).start()
        near(u, 1).start()

    third(0).start()
    for a in range(4):
        for b in range(4):
            if (a, b) != (0, 0):
                if b > 0:
                    second(0, a, b).wait_recv()
                if a > 0:
                    second(1, b, a).wait_recv()
                third(a * 4 + b).start()
    swap.wait_recv()
    for k in range(16):
        third(k).wait_recv()

    row, col = iota((16, nq), 0), iota((16, nq), 1)
    sel = jnp.where((row < 3 * heads) & (row % heads == col // half), 1.0, 0.0).astype(BF16)
    qs[0] = jnp.concatenate([qo[0], sel], axis=0)
    qs[1] = jnp.concatenate([qf[...], sel], axis=0)
    m_s[...] = jnp.full(m_s.shape, NEG_FILL, F32)
    acc[...] = jnp.zeros(acc.shape, F32)
    hidden_keys = iota((half, half), 0) > iota((half, half), 1)

    def place(n):
        late = n >= me
        return jnp.where(late, 1, 0), jnp.where(late, n - me, n)

    def scores(hf, kb, s_ref, mode="full"):
        keys = jnp.concatenate([kv[kb, 0:HD, :].astype(F32), gs[kb]], axis=0)
        keys = jnp.transpose(keys).astype(BF16)
        for pt in [0] if mode == "first" else [0, 1]:
            for h in range(heads):
                cols = slice(h * half, (h + 1) * half)
                s = dot(keys[pt * half : (pt + 1) * half], qs[hf, :, cols])
                if mode == "first" or (mode == "second" and pt == 1):
                    s = jnp.where(hidden_keys, NEG_FILL, s)
                s_ref[pt * half : (pt + 1) * half, cols] = s

    def weigh(hf, kb, s_ref, mode="full"):
        count = half if mode == "first" else 2 * half
        vals = jnp.concatenate([kv[kb, HD : 2 * HD, 0:count], jnp.ones((16, count), BF16)], axis=0)
        for h in range(heads):
            cols = slice(h * half, (h + 1) * half)
            top = m_s[hf, 0:1, cols]
            new = jnp.maximum(top, jnp.max(s_ref[0:count, cols], axis=0, keepdims=True))
            weight = jnp.exp(s_ref[0:count, cols] - new).astype(BF16)
            m_s[hf, 0:1, cols] = new
            acc[hf, :, cols] = acc[hf, :, cols] * jnp.exp(top - new) + dot(vals, weight)

    scores(0, me, s_a, "first")
    scores(1, mirror, s_b, "second")
    weigh(0, me, s_a, "first")
    scores(*place(0), s_a)
    weigh(1, mirror, s_b, "second")

    def attend(t):
        n = 2 * t
        scores(*place(n + 1), s_b)
        weigh(*place(n), s_a)
        scores(*place(n + 2), s_a)
        weigh(*place(n + 1), s_b)

    pl.loop(0, (experts - 2) // 2)(attend)
    weigh(*place(experts - 2), s_a)

    for hf in range(2):
        o = (acc[hf, 0:HD, :] / acc[hf, HD : HD + 1, :]).astype(BF16)
        for q in range(2):
            for h in range(heads):
                ob[hf, q, h * HD : (h + 1) * HD, :] = o[
                    :, h * half + q * (half // 2) : h * half + (q + 1) * (half // 2)
                ]

    def deliver(hf, q):
        return send(
            ob.at[hf, q], mx.at[p], ob_ss.at[hf, q], ob_rs.at[p], me if hf == 0 else mirror, 2 * hf + q
        )

    for q in range(2):
        deliver(1, q).start()

        @pl.when(p == q)
        def _():
            mx[q] = ob[0, q]

        @pl.when(p != q)
        def _():
            deliver(0, q).start()

    def give(r):
        return send(res.at[r], ret.at[me], ret_ss.at[r], ret_rs.at[r], away(r, -1), p)

    @pl.loop(0, 2)
    def _(u):
        near(u, 0).wait_recv()
        near(u, 1).wait_recv()
        part = pl.ds(u * upper, upper)
        total = own[part].astype(F32) + near_r[0, part].astype(F32) + near_r[1, part].astype(F32)
        res[part] = total.astype(BF16)

        @pl.loop(jnp.where(u == 0, 1, upper), (u + 1) * upper)
        def _(r):
            give(r).start()

    ret[me] = res[0]

    weights[3].wait()

    def arrived(k):
        return send(ob.at[0, 0], mx.at[k], ob_ss.at[0, 0], ob_rs.at[k], me, p)

    for k in range(4):

        @pl.when(p != k)
        def _():
            arrived(k).wait_recv()

        if k >= 2:

            @pl.when(p == k)
            def _():
                arrived(k).wait_recv()

    projected = dot_t(mx[...].reshape(4 * heads * HD, half // 2), wo[...])
    mix_out[...] = norm_rows(projected, apost_ref[...]).astype(BF16)

    start = pl.multiple_of(p * quarter, quarter)
    own_ids = ids_ref[pl.ds(start, quarter), :]
    own_rw = rw_ref[pl.ds(start, quarter), :]
    each = iota((quarter, experts), 1)
    hit = [own_ids[:, k : k + 1] == each for k in range(TOP_K)]
    lower = (iota((quarter, quarter), 0) > iota((quarter, quarter), 1)).astype(F32).astype(BF16)
    ranks = dot(lower, (hit[0] | hit[1]).astype(F32).astype(BF16))
    slot = iota((quarter, experts * SLOT), 1)
    picks = []
    for k in range(TOP_K):
        rank = jnp.sum(jnp.where(hit[k], ranks, 0.0), axis=1, keepdims=True)
        want = own_ids[:, k : k + 1] * SLOT + rank.astype(jnp.int32)
        picks.append((slot == want).astype(F32).astype(BF16))

    @pl.loop(1, experts)
    def _(r):
        give(r).wait_recv()

    rows_back = ret[...].reshape(experts * SLOT, width)
    combined = jnp.zeros((quarter, width), F32)
    for k in range(TOP_K):
        combined = combined + own_rw[:, k : k + 1] * dot(picks[k], rows_back)
    exp_out[...] = norm_rows(combined, mpost_ref[...]).astype(BF16)

    @pl.loop(1, experts)
    def _(r):
        disp(r, away(r, 1)).wait_send()
        give(r).wait_send()

    @pl.loop(0, experts)
    def _(r):
        fwd(r).wait_send()

    @pl.loop(0, 2)
    def _(u):
        far(u).wait_send()
        near(u, 0).wait_send()
        near(u, 1).wait_send()

    swap.wait_send()
    for part in range(2):
        for d in range(1, 4):
            first(part, d).wait_send()
            for a in range(4):
                second(part, a, d).wait_send()
    for k in range(16):
        third(k).wait_send()
    for q in range(2):
        deliver(1, q).wait_send()

        @pl.when(p != q)
        def _():
            deliver(0, q).wait_send()


def per_device(*args):
    (x, lf, again, wq, wk, wv, wo, apost, m, ids, rw, mgain, wg, wu, wd, mpost) = args
    rows, width = x.shape
    heads, half = wq.shape[1] // HD, rows // 2
    nq = heads * half
    n_ep, n_tp = lax.axis_size("ep"), lax.axis_size("tp")
    units = wg.shape[2]
    upper = n_ep // 2
    tokens = m.shape[0]
    vmem = pl.BlockSpec(memory_space=pltpu.VMEM)
    hbm = pl.BlockSpec(memory_space=pl.ANY)
    dma = pltpu.SemaphoreType.DMA
    row = lambda a: a.reshape(1, -1)
    return pl.pallas_call(
        whole_kernel,
        out_shape=(
            jax.ShapeDtypeStruct((rows // n_tp, width), BF16),
            jax.ShapeDtypeStruct((tokens // n_tp, width), BF16),
        ),
        in_specs=[vmem] * 6 + [hbm, vmem] + [vmem] * 4 + [hbm] * 3 + [vmem],
        out_specs=(vmem, vmem),
        scratch_shapes=[
            pltpu.VMEM((width, units), BF16),
            pltpu.VMEM((width, units), BF16),
            pltpu.VMEM((units, width), BF16),
            pltpu.VMEM(wo.shape, BF16),
            dma((4,)),
            pltpu.VMEM((n_ep, 2, SLOT, width), BF16),
            pltpu.VMEM((2, n_ep, 2, SLOT, width), BF16),
            pltpu.VMEM((upper, 2, SLOT, width), F32),
            pltpu.VMEM((n_ep, SLOT, width), BF16),
            pltpu.VMEM((2, upper, SLOT, width), BF16),
            pltpu.VMEM((2, upper, SLOT, width), BF16),
            pltpu.VMEM((2, 2, upper, SLOT, width), BF16),
            pltpu.VMEM((2, n_ep, SLOT, width), BF16),
            pltpu.VMEM((n_ep, SLOT, width), BF16),
            pltpu.VMEM((n_ep, SLOT, width), BF16),
            pltpu.VMEM((n_ep, 2 * HD, rows), BF16),
            pltpu.VMEM((2, HD, nq), BF16),
            pltpu.VMEM((HD, nq), BF16),
            pltpu.VMEM((n_ep, 16, rows), F32),
            pltpu.VMEM((2, HD + 16, nq), BF16),
            pltpu.VMEM((2, 8, nq), F32),
            pltpu.VMEM((2, HD + 16, nq), F32),
            pltpu.VMEM((2 * half, nq), F32),
            pltpu.VMEM((2 * half, nq), F32),
            pltpu.VMEM((2, 2, heads * HD, half // 2), BF16),
            pltpu.VMEM((4, heads * HD, half // 2), BF16),
            dma((n_ep,)), dma((n_ep,)), dma((n_ep,)), dma((n_ep,)),
            dma((2,)), dma((2,)), dma((2, 2)), dma((2, 2)), dma((n_ep,)), dma((n_ep,)),
            dma((2,)), dma((2, 4)), dma((2, 4)), dma((2, 4, 4)), dma((2, 4, 4)),
            dma((16,)), dma((16,)), dma((2, 2)), dma((4,)),
        ],
        compiler_params=pltpu.CompilerParams(
            has_side_effects=True, vmem_limit_bytes=67_043_328
        ),
        name="whole",
    )(x, lf, row(again), wq, wk, wv, wo, row(apost), m, ids, rw, row(mgain), wg, wu, wd, row(mpost))


def solution(mesh):
    placed = (
        P("ep", None),
        P("tp", None),
        P(),
        P(None, "tp"),
        P(None, "tp"),
        P(None, "tp"),
        P(),
        P(),
        P("ep", None),
        P("ep", None),
        P("ep", None),
        P(),
        P("ep", None, "tp"),
        P("ep", None, "tp"),
        P("ep", "tp", None),
        P(),
    )
    return jax.shard_map(
        per_device,
        mesh=mesh,
        in_specs=placed,
        out_specs=(P(("ep", "tp"), None), P(("ep", "tp"), None)),
        check_vma=False,
    )
```

time: 232 us -> 129 us (0.56)
  waiting for transfers between devices: 72.2 us -> 0 us
  Pallas kernels: 55.1 us -> 117 us
  starting transfers between devices: 25.6 us -> 0 us
  matrix products: 24 us -> 0 us
  between operations: 15.9 us -> 0.64 us
  local copies, waits for them, and re-layouts: 25.5 us -> 10.4 us
  other arithmetic: 11 us -> 0 us
    all_to_all x3 -> x0, waiting for transfers between devices: 65.6 us -> none  [the longest x1 48.3 us: expert_half(): lax.all_to_all(outgoing, 'ep', split_axis=1, concat_axis=1, tiled=True)]
    pallas_call x1, Pallas kernels: 55.1 us -> 117 us  [per_device(): pl.pallas_call(whole_kernel, out_shape=(jax.ShapeDtypeStruct((rows // n_t...]
    dot_general x11 -> x0, matrix products: 24 us -> none  [the longest x9 22.5 us: dot(): return jnp.dot(a, b, preferred_element_type=F32)]
    all_to_all x3 -> x0, starting transfers between devices: 18.4 us -> none  [the longest x1 8.83 us: expert_half(): lax.all_to_all(outgoing, 'ep', split_axis=1, concat_axis=1, tiled=True)]
    ppermute x2 -> x0, starting transfers between devices: 7.19 us -> none  [the longest x1 5.3 us: mixer_half(): far = lax.ppermute(qt[1], 'ep', swap)]
    ppermute x2 -> x0, waiting for transfers between devices: 6.59 us -> none  [the longest x1 6.59 us: mixer_half(): far_out = lax.ppermute(out[1], 'ep', swap)]
    all_gather x1 -> x0, local copies, waits for them, and re-layouts: 6.41 us -> none  [mixer_half(): kv = lax.all_gather(kv_own, 'ep', axis=0, tiled=False)]
    convert_element_type x6 -> x0, other arithmetic: 5.59 us -> none  [the longest x1 2.14 us: mixer_half(): normed = norm_rows(mixer_input, mixer_gain).astype(BF16)]
  transfers between devices with their start and end apart: 7 -> 0, of which waited for: 4 -> 0; matrix products, arithmetic and copies ran while one was open for 21% -> 0% of each run, Pallas kernels for 24% -> 0%
where the time goes in v2:
time: 129 us; the launch traced here: 128 us
  Pallas kernels  117 us (91%)
  local copies, waits for them, and re-layouts  10.4 us (8%)
    pallas_call x1, Pallas kernels, per_device(): pl.pallas_call(whole_kernel, out_shape=(jax.ShapeDtypeStruct((rows // n_t...  117 us
    unnamed x6, local copies, waits for them, and re-layouts  10.4 us

profile of v2, /device:TPU:7, one launch (start us, length us, event | category | flops | bytes accessed | tf_op | source)
XLA Modules:
  0.0 128.3 jit_solution(11414477126930702574)
XLA Ops:
  0.6 1.5 %copy.20.ids_ref = s32[256,2]{1,0:T(8,128)} copy(s32[256,2]{0,1:T(2,128)} %param.25) | data formatting | bytes 4096 | tf_op args[9]
  2.1 1.5 %copy.21.rw_ref = f32[256,2]{1,0:T(8,128)} copy(f32[256,2]{0,1:T(2,128)} %param.26) | data formatting | bytes 4096 | tf_op args[10]
  3.6 2.0 %copy.18.wk_ref = bf16[2048,64]{1,0:T(8,128)(2,1)} copy(bf16[2048,64]{0,1:T(8,128)(2,1)} %param.20) | data formatting | bytes 524288 | tf_op args[4]
  5.5 1.9 %copy.19.wv_ref = bf16[2048,64]{1,0:T(8,128)(2,1)} copy(bf16[2048,64]{0,1:T(8,128)(2,1)} %param.21) | data formatting | bytes 524288 | tf_op args[5]
  7.5 117.3 %whole.1 = (bf16[128,2048]{1,0:T(8,128)(2,1)}, bf16[64,2048]{1,0:T(8,128)(2,1)}) custom-call(bf16[512,2048]{1,0:T(8,128)(2,1)} %x_ref.1, f32[4,16384]{1,0:T(4,128)} %lf_ref.1, f32[1,2048]{1,0:T(1,128)} %bitcast.4, bf16[2048,256]{1,0:T(8,128)(2,1)} %wq_ref.1, bf16[2048,64]{1,0:T(8,128)(2,1)} %copy.18.wk_ref, bf16[2048,64]{1,0:T(8,128)(2,1)} %copy.19.wv_ref, ...), custom_call_target="tpu_custom_call" | custom-call | tf_op jit(solution)/shard_map/whole/pallas_call | solution.py:425
  124.7 1.9 %copy.24 = bf16[128,2048]{1,0:T(8,128)(2,1)} copy(bf16[128,2048]{1,0:T(8,128)(2,1)} %get-tuple-element.4) | data formatting | bytes 1048576
  126.6 1.7 %copy.25 = bf16[64,2048]{1,0:T(8,128)(2,1)} copy(bf16[64,2048]{1,0:T(8,128)(2,1)} %get-tuple-element.5) | data formatting | bytes 524288

commit v3 on v2

--- a/solution.py
+++ b/solution.py
@@ -14,6 +14,8 @@
 F32 = jnp.float32
 BF16 = jnp.bfloat16
 SLOT = 8
+SPLIT = 8
+FINISH = 4
 
 
 def norm_rows(values_in, gain_vec):
@@ -38,10 +40,10 @@
 
 
 def whole_kernel(
-    x_ref, lf_ref, again_ref, wq_ref, wk_ref, wv_ref, wo_hbm, apost_ref,
-    m_ref, ids_ref, rw_ref, mgain_ref, wg_hbm, wu_hbm, wd_hbm, mpost_ref,
+    x_hbm, lf_ref, again_ref, wq_hbm, wk_hbm, wv_hbm, wo_hbm, apost_ref,
+    m_hbm, ids_ref, rw_ref, mgain_ref, wg_hbm, wu_hbm, wd_hbm, mpost_ref,
     mix_out, exp_out,
-    wg, wu, wd, wo, w_sem,
+    x_ref, wq_ref, wk_ref, m_ref, wg, wu, wd, wo, w_sem,
     outgoing, arr, prod, own, far_s, far_r, near_s, near_r, res, ret,
     kv, qo, qf, gs, qs, m_s, acc, s_a, s_b, ob, mx,
     disp_ss, disp_rs, fwd_ss, fwd_rs, far_ss, far_rs, near_ss, near_rs, ret_ss, ret_rs,
@@ -52,12 +54,12 @@
     z, y, c = me // 8, (me // 2) % 4, me % 2
     mirror = 31 - me
     parity = p % 2
-    rows = x_ref.shape[0]
+    rows = x_hbm.shape[0]
     half = rows // 2
-    heads = wq_ref.shape[1] // HD
+    heads = wq_hbm.shape[1] // HD
     nq = heads * half
-    width = x_ref.shape[1]
-    tokens = m_ref.shape[0]
+    width = x_hbm.shape[1]
+    tokens = m_hbm.shape[0]
     quarter = tokens // 4
     experts = arr.shape[1]
     upper = experts // 2
@@ -79,23 +81,50 @@
             device_id_type=pl.DeviceIdType.MESH,
         )
 
-    weights = [
-        pltpu.make_async_copy(a, b, w_sem.at[k])
-        for k, (a, b) in enumerate(((wg_hbm.at[0], wg), (wu_hbm.at[0], wu), (wd_hbm.at[0], wd), (wo_hbm, wo)))
+    loads = [
+        pltpu.make_async_copy(src, dst, w_sem.at[k])
+        for k, (src, dst) in enumerate(
+            (
+                (m_hbm, m_ref),
+                (x_hbm, x_ref),
+                (wk_hbm, wk_ref.at[0:HD]),
+                (wv_hbm, wk_ref.at[HD : 2 * HD]),
+                (wq_hbm, wq_ref),
+                (wg_hbm.at[0], wg),
+                (wu_hbm.at[0], wu),
+                (wd_hbm.at[0], wd),
+                (wo_hbm, wo),
+            )
+        )
     ]
-    for w in weights:
-        w.start()
-
-    normed_m = norm_rows(m_ref[...], mgain_ref[...]).astype(BF16)
-    each = iota((tokens, experts), 1)
-    chosen = ((ids_ref[:, 0:1] == each) | (ids_ref[:, 1:2] == each)).astype(F32).astype(BF16)
+    for load in loads:
+        load.start()
+
+    barrier = pltpu.get_barrier_semaphore()
+
+    def greet(ep, tp):
+        pl.semaphore_signal(
+            barrier, inc=1, device_id={"ep": ep, "tp": tp}, device_id_type=pl.DeviceIdType.MESH
+        )
+
+    @pl.loop(1, experts)
+    def _(r):
+        greet(away(r, 1), p)
+
+    for d in range(1, 4):
+        greet(me, (p + d) % 4)
+        greet(mirror, (p + d) % 4)
+
+    each = iota((experts, tokens), 0)
+    named = [ids_ref[k : k + 1, :] == each for k in range(TOP_K)]
+    chosen = named[0] | named[1]
     t_row, t_col = iota((tokens, tokens), 0), iota((tokens, tokens), 1)
     before = ((t_row // quarter == t_col // quarter) & (t_row < t_col)).astype(F32).astype(BF16)
-    same = (t_row == t_col).astype(F32).astype(BF16)
-    chosen_t = dot_t(chosen, same)
-    ranks_t = dot_t(chosen, before)
-    ranks_t = jnp.where(chosen_t > 0.5, ranks_t, -1.0)
+    ranks = dot(chosen.astype(F32).astype(BF16), before)
+    ranks_t = jnp.where(chosen, ranks, -1.0)
     block_of = iota((experts, tokens), 1) // quarter
+    loads[0].wait()
+    normed_m = norm_rows(m_ref[...], mgain_ref[...]).astype(BF16)
     for hb in range(2):
         mine = jnp.where(block_of == parity + 2 * hb, ranks_t, -1.0)
         wide = jnp.broadcast_to(mine[:, None, :], (experts, SLOT, tokens))
@@ -112,16 +141,12 @@
             arr.at[0, r], arr.at[1, r], fwd_ss.at[r], fwd_rs.at[r], me, (p + 1 + 2 * (r % 2)) % 4
         )
 
-    @pl.loop(1, experts)
-    def _(r):
-        disp(r, away(r, 1)).start()
-
-    arr[0, 0] = outgoing[me]
-
+    for load in loads[1:5]:
+        load.wait()
     normed_a = norm_rows(x_ref[...], again_ref[...]).astype(BF16)
-    kt = dot(normed_a, wk_ref[...]).astype(BF16).astype(F32)
-    vt = dot(normed_a, wv_ref[...]).astype(BF16).astype(F32)
-    kv[me] = jnp.transpose(jnp.concatenate([kt, vt], axis=1)).astype(BF16)
+    kv[me] = lax.dot_general(
+        wk_ref[...], normed_a, (((1,), (1,)), ((), ())), preferred_element_type=F32
+    ).astype(BF16)
     qt = dot(normed_a, wq_ref[...]).astype(BF16).astype(F32) * (HD**-0.5)
     qt = jnp.transpose(qt).astype(BF16)
     for hf in range(2):
@@ -130,7 +155,6 @@
                 h * HD : (h + 1) * HD, hf * half : (hf + 1) * half
             ]
     swap = send(qo.at[1], qf, q_sem.at[0], q_sem.at[1], mirror, p)
-    swap.start()
 
     def first(part, d):
         ref = kv.at[me, part * HD : (part + 1) * HD]
@@ -147,9 +171,17 @@
         ref = kv.at[ep_of(z - k // 4, y - k % 4, c)]
         return send(ref, ref, k3_ss.at[k], k3_rs.at[k], ep_of(z, y, c + 1), p)
 
+    pl.semaphore_wait(barrier, experts - 1 + 6)
     for part in range(2):
         for d in range(1, 4):
             first(part, d).start()
+
+    @pl.loop(1, upper)
+    def _(r):
+        disp(r, away(r, 1)).start()
+
+    swap.start()
+    arr[0, 0] = outgoing[me]
 
     @pl.loop(0, experts)
     def _(kb):
@@ -160,15 +192,24 @@
             rest = rest - piece
         gs[kb, 3 * heads : 16, :] = jnp.zeros((16 - 3 * heads, rows), F32)
 
+    for part in range(2):
+        for a in range(4):
+            if a > 0:
+                first(part, a).wait_recv()
+            for d in range(1, 4):
+                second(part, a, d).start()
+
+    @pl.loop(upper, experts)
+    def _(r):
+        disp(r, away(r, 1)).start()
+
     fwd(0).start()
 
-    @pl.loop(1, experts)
-    def _(r):
-        disp(r, away(r, 1)).wait_recv()
-        fwd(r).start()
-
-    for w in weights[:3]:
-        w.wait()
+    def pass_on(low, high):
+        @pl.loop(low, high)
+        def _(r):
+            disp(r, away(r, 1)).wait_recv()
+            fwd(r).start()
 
     def ffn(v, u):
         rows_in = arr[v, pl.ds(u * upper, upper)].reshape(upper * 2 * SLOT, width)
@@ -182,73 +223,78 @@
                 hidden, wd[:, n * tile : (n + 1) * tile]
             ).reshape(upper, 2, SLOT, tile)
 
-    def far(u):
+    low = upper // 2
+
+    def far(u, h):
+        part = pl.ds(h * low, low)
         return send(
-            far_s.at[u], far_r.at[u], far_ss.at[u], far_rs.at[u], me, (p + 1 + 2 * u) % 4
-        )
-
-    @pl.loop(0, 2)
-    def _(u):
+            far_s.at[u, part],
+            far_r.at[u, part],
+            far_ss.at[u, h],
+            far_rs.at[u, h],
+            me,
+            (p + 1 + 2 * h) % 4,
+        )
+
+    def near(u, k, h):
+        return send(
+            near_s.at[u, k, pl.ds(h * low, low)],
+            near_r.at[k, pl.ds(u * upper + h * low, low)],
+            near_ss.at[u, k, h],
+            near_rs.at[u, k, h],
+            me,
+            (p + 1 + 2 * k) % 4,
+        )
+
+    def direct(u):
         ffn(0, u)
+        far_s[u] = prod[:, 1 - p // 2].astype(BF16)
+        far(u, 0).start()
+        far(u, 1).start()
         own[pl.ds(u * upper, upper)] = prod[:, p // 2].astype(BF16)
-        far_s[u] = prod[:, 1 - p // 2].astype(BF16)
-        far(u).start()
-
-    for part in range(2):
-        for a in range(4):
-            if a > 0:
-                first(part, a).wait_recv()
-            for d in range(1, 4):
-                second(part, a, d).start()
 
     plus = ((p + 1) % 4) // 2
 
-    def near(u, k):
-        side = (u + k) % 2
-        return send(
-            near_s.at[u, k],
-            near_r.at[side, pl.ds(u * upper, upper)],
-            near_ss.at[u, side],
-            near_rs.at[u, side],
-            me,
-            (p + 1 + 2 * side) % 4,
-        )
-
-    @pl.loop(0, 2)
-    def _(u):
+    def passed(u):
         @pl.loop(0, upper)
         def _(k):
             fwd(u * upper + k).wait_recv()
 
         ffn(1, u)
-        far(u).wait_recv()
-        joined = (plus + u) % 2
-        near_s[u, 0] = (
-            prod[:, joined].astype(BF16).astype(F32) + far_r[u].astype(F32)
-        ).astype(BF16)
-        near_s[u, 1] = prod[:, 1 - joined].astype(BF16)
-        near(u, 0).start()
-        near(u, 1).start()
-
-    third(0).start()
-    for a in range(4):
-        for b in range(4):
-            if (a, b) != (0, 0):
-                if b > 0:
-                    second(0, a, b).wait_recv()
-                if a > 0:
-                    second(1, b, a).wait_recv()
-                third(a * 4 + b).start()
-    swap.wait_recv()
-    for k in range(16):
-        third(k).wait_recv()
-
-    row, col = iota((16, nq), 0), iota((16, nq), 1)
-    sel = jnp.where((row < 3 * heads) & (row % heads == col // half), 1.0, 0.0).astype(BF16)
-    qs[0] = jnp.concatenate([qo[0], sel], axis=0)
-    qs[1] = jnp.concatenate([qf[...], sel], axis=0)
-    m_s[...] = jnp.full(m_s.shape, NEG_FILL, F32)
-    acc[...] = jnp.zeros(acc.shape, F32)
+        for k in range(2):
+            h = 1 - k
+            near_s[u, k, h * low : (h + 1) * low] = prod[
+                h * low : (h + 1) * low, (plus + k) % 2
+            ].astype(BF16)
+            near(u, k, h).start()
+        for k in range(2):
+            far(u, k).wait_recv()
+            half_of = slice(k * low, (k + 1) * low)
+            near_s[u, k, half_of] = (
+                prod[half_of, (plus + k) % 2].astype(BF16).astype(F32)
+                + far_r[u, half_of].astype(F32)
+            ).astype(BF16)
+            near(u, k, k).start()
+
+    pass_on(1, upper)
+    for load in loads[5:8]:
+        load.wait()
+
+    def give(r):
+        return send(res.at[r], ret.at[me], ret_ss.at[r], ret_rs.at[r], away(r, -1), p)
+
+    def finish(u):
+        for k in range(2):
+            for h in range(2):
+                near(u, k, h).wait_recv()
+        part = pl.ds(u * upper, upper)
+        total = own[part].astype(F32) + near_r[0, part].astype(F32) + near_r[1, part].astype(F32)
+        res[part] = total.astype(BF16)
+
+        @pl.loop(max(1, u * upper), (u + 1) * upper)
+        def _(r):
+            give(r).start()
+
     hidden_keys = iota((half, half), 0) > iota((half, half), 1)
 
     def place(n):
@@ -277,12 +323,6 @@
             m_s[hf, 0:1, cols] = new
             acc[hf, :, cols] = acc[hf, :, cols] * jnp.exp(top - new) + dot(vals, weight)
 
-    scores(0, me, s_a, "first")
-    scores(1, mirror, s_b, "second")
-    weigh(0, me, s_a, "first")
-    scores(*place(0), s_a)
-    weigh(1, mirror, s_b, "second")
-
     def attend(t):
         n = 2 * t
         scores(*place(n + 1), s_b)
@@ -290,7 +330,53 @@
         scores(*place(n + 2), s_a)
         weigh(*place(n + 1), s_b)
 
-    pl.loop(0, (experts - 2) // 2)(attend)
+    blocks = (experts - 2) // 2
+
+    @pl.loop(0, 2)
+    def _(u):
+        direct(u)
+        passed(u)
+
+        @pl.when(u == 0)
+        def _():
+            third(0).start()
+            for a in range(4):
+                for b in range(4):
+                    if (a, b) != (0, 0):
+                        if b > 0:
+                            second(0, a, b).wait_recv()
+                        if a > 0:
+                            second(1, b, a).wait_recv()
+                        third(a * 4 + b).start()
+            swap.wait_recv()
+            for k in range(16):
+                third(k).wait_recv()
+
+            row, col = iota((16, nq), 0), iota((16, nq), 1)
+            sel = jnp.where((row < 3 * heads) & (row % heads == col // half), 1.0, 0.0).astype(BF16)
+            qs[0] = jnp.concatenate([qo[0], sel], axis=0)
+            qs[1] = jnp.concatenate([qf[...], sel], axis=0)
+            m_s[...] = jnp.full(m_s.shape, NEG_FILL, F32)
+            acc[...] = jnp.zeros(acc.shape, F32)
+            scores(0, me, s_a, "first")
+            scores(1, mirror, s_b, "second")
+            weigh(0, me, s_a, "first")
+            scores(*place(0), s_a)
+            weigh(1, mirror, s_b, "second")
+
+
+        @pl.loop(u * SPLIT, jnp.where(u == 0, SPLIT, blocks))
+        def _(t):
+            attend(t)
+
+            @pl.when(u == 0)
+            def _():
+                pass_on(upper + t * upper // SPLIT, upper + (t + 1) * upper // SPLIT)
+
+            @pl.when(t == FINISH)
+            def _():
+                finish(0)
+
     weigh(*place(experts - 2), s_a)
 
     for hf in range(2):
@@ -317,24 +403,10 @@
         def _():
             deliver(0, q).start()
 
-    def give(r):
-        return send(res.at[r], ret.at[me], ret_ss.at[r], ret_rs.at[r], away(r, -1), p)
-
-    @pl.loop(0, 2)
-    def _(u):
-        near(u, 0).wait_recv()
-        near(u, 1).wait_recv()
-        part = pl.ds(u * upper, upper)
-        total = own[part].astype(F32) + near_r[0, part].astype(F32) + near_r[1, part].astype(F32)
-        res[part] = total.astype(BF16)
-
-        @pl.loop(jnp.where(u == 0, 1, upper), (u + 1) * upper)
-        def _(r):
-            give(r).start()
-
+    finish(1)
     ret[me] = res[0]
 
-    weights[3].wait()
+    loads[8].wait()
 
     def arrived(k):
         return send(ob.at[0, 0], mx.at[k], ob_ss.at[0, 0], ob_rs.at[k], me, p)
@@ -354,19 +426,18 @@
     projected = dot_t(mx[...].reshape(4 * heads * HD, half // 2), wo[...])
     mix_out[...] = norm_rows(projected, apost_ref[...]).astype(BF16)
 
-    start = pl.multiple_of(p * quarter, quarter)
-    own_ids = ids_ref[pl.ds(start, quarter), :]
-    own_rw = rw_ref[pl.ds(start, quarter), :]
-    each = iota((quarter, experts), 1)
-    hit = [own_ids[:, k : k + 1] == each for k in range(TOP_K)]
-    lower = (iota((quarter, quarter), 0) > iota((quarter, quarter), 1)).astype(F32).astype(BF16)
-    ranks = dot(lower, (hit[0] | hit[1]).astype(F32).astype(BF16))
-    slot = iota((quarter, experts * SLOT), 1)
-    picks = []
+    mine = (iota((tokens, quarter), 0) == p * quarter + iota((tokens, quarter), 1)).astype(F32).astype(BF16)
+    own_ranks = dot(ranks.astype(BF16), mine)
+    mine_t = iota((quarter, tokens), 1) == p * quarter + iota((quarter, tokens), 0)
+    picks, shares = [], []
     for k in range(TOP_K):
-        rank = jnp.sum(jnp.where(hit[k], ranks, 0.0), axis=1, keepdims=True)
-        want = own_ids[:, k : k + 1] * SLOT + rank.astype(jnp.int32)
-        picks.append((slot == want).astype(F32).astype(BF16))
+        hit = dot(named[k].astype(F32).astype(BF16), mine)
+        want = jnp.where(hit > 0.5, own_ranks, -1.0)
+        wide = jnp.broadcast_to(want[:, None, :], (experts, SLOT, quarter))
+        table = jnp.where(wide == iota((experts, SLOT, quarter), 1).astype(F32), 1.0, 0.0)
+        picks.append(table.reshape(experts * SLOT, quarter).astype(BF16))
+        share = jnp.where(mine_t, rw_ref[k : k + 1, :], 0.0)
+        shares.append(jnp.sum(share, axis=1, keepdims=True))
 
     @pl.loop(1, experts)
     def _(r):
@@ -375,7 +446,7 @@
     rows_back = ret[...].reshape(experts * SLOT, width)
     combined = jnp.zeros((quarter, width), F32)
     for k in range(TOP_K):
-        combined = combined + own_rw[:, k : k + 1] * dot(picks[k], rows_back)
+        combined = combined + shares[k] * dot_t(picks[k], rows_back)
     exp_out[...] = norm_rows(combined, mpost_ref[...]).astype(BF16)
 
     @pl.loop(1, experts)
@@ -389,9 +460,10 @@
 
     @pl.loop(0, 2)
     def _(u):
-        far(u).wait_send()
-        near(u, 0).wait_send()
-        near(u, 1).wait_send()
+        for k in range(2):
+            far(u, k).wait_send()
+            for h in range(2):
+                near(u, k, h).wait_send()
 
     swap.wait_send()
     for part in range(2):
@@ -428,14 +500,18 @@
             jax.ShapeDtypeStruct((rows // n_tp, width), BF16),
             jax.ShapeDtypeStruct((tokens // n_tp, width), BF16),
         ),
-        in_specs=[vmem] * 6 + [hbm, vmem] + [vmem] * 4 + [hbm] * 3 + [vmem],
+        in_specs=[hbm, vmem, vmem] + [hbm] * 4 + [vmem, hbm] + [vmem] * 3 + [hbm] * 3 + [vmem],
         out_specs=(vmem, vmem),
         scratch_shapes=[
+            pltpu.VMEM(x.shape, BF16),
+            pltpu.VMEM(wq.shape, BF16),
+            pltpu.VMEM((2 * HD, width), BF16),
+            pltpu.VMEM(m.shape, BF16),
             pltpu.VMEM((width, units), BF16),
             pltpu.VMEM((width, units), BF16),
             pltpu.VMEM((units, width), BF16),
             pltpu.VMEM(wo.shape, BF16),
-            dma((4,)),
+            dma((9,)),
             pltpu.VMEM((n_ep, 2, SLOT, width), BF16),
             pltpu.VMEM((2, n_ep, 2, SLOT, width), BF16),
             pltpu.VMEM((upper, 2, SLOT, width), F32),
@@ -458,15 +534,15 @@
             pltpu.VMEM((2, 2, heads * HD, half // 2), BF16),
             pltpu.VMEM((4, heads * HD, half // 2), BF16),
             dma((n_ep,)), dma((n_ep,)), dma((n_ep,)), dma((n_ep,)),
-            dma((2,)), dma((2,)), dma((2, 2)), dma((2, 2)), dma((n_ep,)), dma((n_ep,)),
+            dma((2, 2)), dma((2, 2)), dma((2, 2, 2)), dma((2, 2, 2)), dma((n_ep,)), dma((n_ep,)),
             dma((2,)), dma((2, 4)), dma((2, 4)), dma((2, 4, 4)), dma((2, 4, 4)),
             dma((16,)), dma((16,)), dma((2, 2)), dma((4,)),
         ],
         compiler_params=pltpu.CompilerParams(
-            has_side_effects=True, vmem_limit_bytes=67_043_328
+            collective_id=0, has_side_effects=True, vmem_limit_bytes=67_043_328
         ),
         name="whole",
-    )(x, lf, row(again), wq, wk, wv, wo, row(apost), m, ids, rw, row(mgain), wg, wu, wd, row(mpost))
+    )(x, lf, row(again), wq, wk.T, wv.T, wo, row(apost), m, ids.T, rw.T, row(mgain), wg, wu, wd, row(mpost))
 
 
 def solution(mesh):

time: 129 us -> 108 us (0.84)
  Pallas kernels: 117 us -> 103 us
  local copies, waits for them, and re-layouts: 10.4 us -> 3.55 us
    pallas_call x1, Pallas kernels: 117 us -> 103 us  [per_device(): pl.pallas_call(whole_kernel, out_shape=(jax.ShapeDtypeStruct((rows // n_t...]
    unnamed x6 -> x2, local copies, waits for them, and re-layouts: 10.4 us -> 3.55 us
where the time goes in v3:
time: 108 us; the launch traced here: 107 us
  Pallas kernels  103 us (95%)
  local copies, waits for them, and re-layouts  3.55 us (3%)
    pallas_call x1, Pallas kernels, per_device(): pl.pallas_call(whole_kernel, out_shape=(jax.ShapeDtypeStruct((rows // n_t...  103 us
    unnamed x2, local copies, waits for them, and re-layouts  3.55 us

profile of v3, /device:TPU:7, one launch (start us, length us, event | category | flops | bytes accessed | tf_op | source)
XLA Modules:
  0.0 107.3 jit_solution(15848027052534971118)
XLA Ops:
  0.6 103.1 %whole.1 = (bf16[128,2048]{1,0:T(8,128)(2,1)}, bf16[64,2048]{1,0:T(8,128)(2,1)}) custom-call(bf16[512,2048]{1,0:T(8,128)(2,1)} %x_hbm.1, f32[4,16384]{1,0:T(4,128)} %lf_ref.1, f32[1,2048]{1,0:T(1,128)} %bitcast.10, bf16[2048,256]{1,0:T(8,128)(2,1)} %wq_hbm.1, bf16[64,2048]{1,0:T(8,128)(2,1)} %bitcast.8, bf16[64,2048]{1,0:T(8,128)(2,1)} %bitcast.9, ...), custom_call_target="tpu_custom_call" | custom-call | tf_op jit(solution)/shard_map/whole/pallas_call | solution.py:497
  103.7 1.9 %copy.20 = bf16[128,2048]{1,0:T(8,128)(2,1)} copy(bf16[128,2048]{1,0:T(8,128)(2,1)} %get-tuple-element.4) | data formatting | bytes 1048576
  105.6 1.7 %copy.21 = bf16[64,2048]{1,0:T(8,128)(2,1)} copy(bf16[64,2048]{1,0:T(8,128)(2,1)} %get-tuple-element.5) | data formatting | bytes 524288

commit v4 on v3

--- a/solution.py
+++ b/solution.py
@@ -14,8 +14,12 @@
 F32 = jnp.float32
 BF16 = jnp.bfloat16
 SLOT = 8
-SPLIT = 8
-FINISH = 4
+PIECES = 4
+FIRST = 1
+STARTS = (0, 0, 7, 10)
+JOINS = (0, 0, 10, 14)
+PUMP = 4
+FINISH = (3, 9, 13)
 
 
 def norm_rows(values_in, gain_vec):
@@ -62,7 +66,8 @@
     tokens = m_hbm.shape[0]
     quarter = tokens // 4
     experts = arr.shape[1]
-    upper = experts // 2
+    upper = experts // PIECES
+    middle = experts // 2
 
     def ep_of(a, b, d):
         return ((a + 8) % 4) * 8 + ((b + 8) % 4) * 2 + (d + 2) % 2
@@ -176,7 +181,7 @@
         for d in range(1, 4):
             first(part, d).start()
 
-    @pl.loop(1, upper)
+    @pl.loop(1, middle)
     def _(r):
         disp(r, away(r, 1)).start()
 
@@ -199,7 +204,7 @@
             for d in range(1, 4):
                 second(part, a, d).start()
 
-    @pl.loop(upper, experts)
+    @pl.loop(middle, experts)
     def _(r):
         disp(r, away(r, 1)).start()
 
@@ -267,6 +272,8 @@
                 h * low : (h + 1) * low, (plus + k) % 2
             ].astype(BF16)
             near(u, k, h).start()
+
+    def join(u):
         for k in range(2):
             far(u, k).wait_recv()
             half_of = slice(k * low, (k + 1) * low)
@@ -332,12 +339,23 @@
 
     blocks = (experts - 2) // 2
 
-    @pl.loop(0, 2)
+    def by_piece(u, values):
+        out = values[-1]
+        for k, v in enumerate(values[:-1]):
+            out = jnp.where(u == k, v, out)
+        return out
+
+    @pl.loop(0, PIECES)
     def _(u):
         direct(u)
+
+        @pl.when(u == 0)
+        def _():
+            pass_on(upper, middle)
+
         passed(u)
 
-        @pl.when(u == 0)
+        @pl.when(u == FIRST)
         def _():
             third(0).start()
             for a in range(4):
@@ -365,17 +383,24 @@
             weigh(1, mirror, s_b, "second")
 
 
-        @pl.loop(u * SPLIT, jnp.where(u == 0, SPLIT, blocks))
-        def _(t):
-            attend(t)
-
-            @pl.when(u == 0)
-            def _():
-                pass_on(upper + t * upper // SPLIT, upper + (t + 1) * upper // SPLIT)
-
-            @pl.when(t == FINISH)
-            def _():
-                finish(0)
+        def attend_from(low_bounds, high_bounds):
+            @pl.loop(by_piece(u, low_bounds), by_piece(u, high_bounds))
+            def _(t):
+                attend(t)
+
+                @pl.when(t < PUMP)
+                def _():
+                    pass_on(middle + t * middle // PUMP, middle + (t + 1) * middle // PUMP)
+
+                for k, at in enumerate(FINISH):
+
+                    @pl.when(t == at)
+                    def _():
+                        finish(k)
+
+        attend_from(STARTS, JOINS)
+        join(u)
+        attend_from(JOINS, STARTS[1:] + ((experts - 2) // 2,))
 
     weigh(*place(experts - 2), s_a)
 
@@ -403,7 +428,7 @@
         def _():
             deliver(0, q).start()
 
-    finish(1)
+    finish(PIECES - 1)
     ret[me] = res[0]
 
     loads[8].wait()
@@ -458,7 +483,7 @@
     def _(r):
         fwd(r).wait_send()
 
-    @pl.loop(0, 2)
+    @pl.loop(0, PIECES)
     def _(u):
         for k in range(2):
             far(u, k).wait_send()
@@ -481,6 +506,17 @@
             deliver(0, q).wait_send()
 
 
+def put_out(a_ref, b_ref, a_out, b_out, sems):
+    copies = [
+        pltpu.make_async_copy(a_ref, a_out, sems.at[0]),
+        pltpu.make_async_copy(b_ref, b_out, sems.at[1]),
+    ]
+    for copy in copies:
+        copy.start()
+    for copy in copies:
+        copy.wait()
+
+
 def per_device(*args):
     (x, lf, again, wq, wk, wv, wo, apost, m, ids, rw, mgain, wg, wu, wd, mpost) = args
     rows, width = x.shape
@@ -488,13 +524,13 @@
     nq = heads * half
     n_ep, n_tp = lax.axis_size("ep"), lax.axis_size("tp")
     units = wg.shape[2]
-    upper = n_ep // 2
+    upper = n_ep // PIECES
     tokens = m.shape[0]
     vmem = pl.BlockSpec(memory_space=pltpu.VMEM)
     hbm = pl.BlockSpec(memory_space=pl.ANY)
     dma = pltpu.SemaphoreType.DMA
     row = lambda a: a.reshape(1, -1)
-    return pl.pallas_call(
+    results = pl.pallas_call(
         whole_kernel,
         out_shape=(
             jax.ShapeDtypeStruct((rows // n_tp, width), BF16),
@@ -516,9 +552,9 @@
             pltpu.VMEM((2, n_ep, 2, SLOT, width), BF16),
             pltpu.VMEM((upper, 2, SLOT, width), F32),
             pltpu.VMEM((n_ep, SLOT, width), BF16),
-            pltpu.VMEM((2, upper, SLOT, width), BF16),
-            pltpu.VMEM((2, upper, SLOT, width), BF16),
-            pltpu.VMEM((2, 2, upper, SLOT, width), BF16),
+            pltpu.VMEM((PIECES, upper, SLOT, width), BF16),
+            pltpu.VMEM((PIECES, upper, SLOT, width), BF16),
+            pltpu.VMEM((PIECES, 2, upper, SLOT, width), BF16),
             pltpu.VMEM((2, n_ep, SLOT, width), BF16),
             pltpu.VMEM((n_ep, SLOT, width), BF16),
             pltpu.VMEM((n_ep, SLOT, width), BF16),
@@ -534,7 +570,7 @@
             pltpu.VMEM((2, 2, heads * HD, half // 2), BF16),
             pltpu.VMEM((4, heads * HD, half // 2), BF16),
             dma((n_ep,)), dma((n_ep,)), dma((n_ep,)), dma((n_ep,)),
-            dma((2, 2)), dma((2, 2)), dma((2, 2, 2)), dma((2, 2, 2)), dma((n_ep,)), dma((n_ep,)),
+            dma((PIECES, 2)), dma((PIECES, 2)), dma((PIECES, 2, 2)), dma((PIECES, 2, 2)), dma((n_ep,)), dma((n_ep,)),
             dma((2,)), dma((2, 4)), dma((2, 4)), dma((2, 4, 4)), dma((2, 4, 4)),
             dma((16,)), dma((16,)), dma((2, 2)), dma((4,)),
         ],
@@ -543,6 +579,14 @@
         ),
         name="whole",
     )(x, lf, row(again), wq, wk.T, wv.T, wo, row(apost), m, ids.T, rw.T, row(mgain), wg, wu, wd, row(mpost))
+    return pl.pallas_call(
+        put_out,
+        out_shape=tuple(jax.ShapeDtypeStruct(r.shape, r.dtype) for r in results),
+        in_specs=[vmem, vmem],
+        out_specs=(hbm, hbm),
+        scratch_shapes=[dma((2,))],
+        name="put_out",
+    )(*results)
 
 
 def solution(mesh):

time: 108 us -> 102 us (0.944)
  local copies, waits for them, and re-layouts: 3.55 us -> 0 us
  Pallas kernels: 103 us -> 101 us
    pallas_call x1, Pallas kernels: 103 us -> 98.6 us  [per_device(): pl.pallas_call(whole_kernel, out_shape=(jax.ShapeDtypeStruct((rows // n_t...]
    unnamed x2 -> x0, local copies, waits for them, and re-layouts: 3.55 us -> none
    pallas_call x0 -> x1, Pallas kernels: none -> 2 us  [per_device(): pl.pallas_call(put_out, out_shape=tuple((jax.ShapeDtypeStruct(r.shape, r....]
where the time goes in v4:
time: 102 us; the launch traced here: 101 us
  Pallas kernels  101 us (99%)
    pallas_call x1, Pallas kernels, per_device(): pl.pallas_call(whole_kernel, out_shape=(jax.ShapeDtypeStruct((rows // n_t...  98.6 us

profile of v4, /device:TPU:7, one launch (start us, length us, event | category | flops | bytes accessed | tf_op | source)
XLA Modules:
  0.0 101.2 jit_solution(2287130658485031947)
XLA Ops:
  0.6 98.6 %whole.1 = (bf16[128,2048]{1,0:T(8,128)(2,1)}, bf16[64,2048]{1,0:T(8,128)(2,1)}) custom-call(bf16[512,2048]{1,0:T(8,128)(2,1)} %x_hbm.1, f32[4,16384]{1,0:T(4,128)} %lf_ref.1, f32[1,2048]{1,0:T(1,128)} %bitcast.10, bf16[2048,256]{1,0:T(8,128)(2,1)} %wq_hbm.1, bf16[64,2048]{1,0:T(8,128)(2,1)} %bitcast.8, bf16[64,2048]{1,0:T(8,128)(2,1)} %bitcast.9, ...), custom_call_target="tpu_custom_call" | custom-call | tf_op jit(solution)/shard_map/whole/pallas_call | solution.py:533
  99.2 2.0 %put_out.1 = (bf16[128,2048]{1,0:T(8,128)(2,1)}, bf16[64,2048]{1,0:T(8,128)(2,1)}) custom-call(bf16[128,2048]{1,0:T(8,128)(2,1)} %get-tuple-element.4.a_ref, bf16[64,2048]{1,0:T(8,128)(2,1)} %get-tuple-element.5.b_ref), custom_call_target="tpu_custom_call" | custom-call | tf_op jit(solution)/shard_map/put_out/pallas_call | solution.py:582
